TPU v7x, 128 devices: a whole 4x4x4 slice. The times are simulated.
128 devices in a mesh: ep: 16 (over z, x), tp: 8 (over y, core).
Axes of the slice: x: 4, y: 4, z: 4, core: 2. Of those that a mesh axis runs over, the one named last changes fastest.
Arguments:
- tokens: bfloat16 [512, 2048], P('ep'), may hold values from -6 to 6
- lengths: int32 [512], P('ep'), may hold values from 128 to 1024, as said below
- cache_keys: bfloat16 [512, 1024, 1024], P('ep', None, 'tp'), may hold values from -140 to 140
- cache_values: bfloat16 [512, 1024, 1024], P('ep', None, 'tp'), may hold values from -6 to 6
- attn_gain: float32 [2048], replicated, may hold values from 0.1 to 1.9
- q_first_w: bfloat16 [2048, 512], P(None, 'tp'), may hold values from -0.19921875 to 0.19921875
- q_second_w: bfloat16 [2048, 512], P(None, 'tp'), may hold values from -0.19921875 to 0.19921875
- k_first_w: bfloat16 [2048, 512], P(None, 'tp'), may hold values from -0.125 to 0.125
- k_second_w: bfloat16 [2048, 512], P(None, 'tp'), may hold values from -0.125 to 0.125
- value_w: bfloat16 [2048, 1024], P(None, 'tp'), may hold values from -0.125 to 0.125
- mix_lambda: float32 [8], P('tp'), may hold values from 0.3 to 0.8
- head_gain: float32 [128], replicated, may hold values from 0.1 to 1.9
- out_w: bfloat16 [1024, 2048], P('tp'), may hold values from -0.09375 to 0.09375
- ffn_gain: float32 [2048], replicated, may hold values from 0.1 to 1.9
- routes: int32 [512, 4], P('ep'), may hold values from 0 to 63, all different within a row; in each aligned block of 32 rows (0 to 31, 32 to 63, ...) at most 4 rows name the same one
- route_logits: float32 [512, 4], P('ep'), may hold values from -4 to 4
- gate_w: bfloat16 [64, 2048, 1024], P('ep', None, 'tp'), may hold values from -0.34960938 to 0.34960938
- up_w: bfloat16 [64, 2048, 1024], P('ep', None, 'tp'), may hold values from -0.34960938 to 0.34960938
- down_w: bfloat16 [64, 1024, 2048], P('ep', None, 'tp'), may hold values from -0.125 to 0.125
Outputs:
- mixed: bfloat16 [512, 2048], P('ep', 'tp')
Inputs may be any that keep to these rules, and one draw needn't show every extreme that they name: `lengths`: at least 128 positions; among the 32 sequences of each index of ep one holds exactly 1024. `routes`: each row names 4 different experts; within the rows of one device no expert is named more than 4 times, a bound that some block reaches.
All inputs are finite; a program needn't handle non-finite values.
Results may differ from a plain program's by a relative error of at most 0.015.
Values may be sent and summed in bfloat16 or wider, within the bound.
A program may use at most 128 MiB of HBM per device.

v0:
```python
import jax
import jax.numpy as jnp
from jax import lax
from jax.sharding import PartitionSpec as P

EPS = 1e-06
LIMIT = 7.0
ALPHA = 1.702


def sent_to_all(x, axis):
    copies = jnp.broadcast_to(x, (lax.axis_size(axis), *x.shape))
    return lax.all_to_all(copies, axis, split_axis=0, concat_axis=0, tiled=True)


def in_order(parts, dim):
    parts = jnp.moveaxis(parts, 0, dim)
    shape = parts.shape
    return parts.reshape(*shape[:dim], shape[dim] * shape[dim + 1], *shape[dim + 2 :])


def gathered_copies(x, axis, dim):
    parts = sent_to_all(x, axis)
    return in_order(parts, dim)


def cut_along(x, dim, count):
    shape = x.shape
    parts = x.reshape(*shape[:dim], count, shape[dim] // count, *shape[dim + 1 :])
    return jnp.moveaxis(parts, dim, 0)


def summed_on_arrival(x, axis, dim):
    parts = cut_along(x, dim, lax.axis_size(axis))
    arrived = lax.all_to_all(parts, axis, split_axis=0, concat_axis=0, tiled=True)
    return arrived.astype(jnp.float32).sum(axis=0)


def over_copies(x, axis):
    return sent_to_all(x, axis).sum(axis=0)


def rms_scale(rows, gain):
    mean_sq = jnp.mean(rows * rows, axis=-1, keepdims=True)
    return rows * lax.rsqrt(mean_sq + EPS) * gain


def slot_tables(routes, weights, expert_ids, capacity):
    blocks, seqs, top = routes.shape
    flat = routes.reshape(blocks, seqs * top)
    order = jnp.arange(seqs * top, dtype=jnp.int32)
    same = (flat[:, None, :] == flat[:, :, None]) & (order[None, None, :] < order[None, :, None])
    rank = jnp.sum(same.astype(jnp.int32), axis=2)
    match = flat[:, :, None] == expert_ids[None, None, :]
    hit = rank[:, :, None] == jnp.arange(capacity, dtype=jnp.int32)[None, None, :]
    table = (match[:, :, :, None] & hit[:, :, None, :]).astype(jnp.float32)
    table = table.reshape(blocks, seqs, top, expert_ids.shape[0], capacity)
    dispatch = jnp.sum(table, axis=2)
    combine = jnp.sum(table * weights[:, :, :, None, None], axis=2)
    return (dispatch, combine)


def attend_heads(
    normed,
    lengths,
    cache_keys,
    cache_values,
    q_first_w,
    q_second_w,
    k_first_w,
    k_second_w,
    value_w,
    mix_lambda,
    head_gain,
):
    seqs = normed.shape[0]
    heads = mix_lambda.shape[0]
    width = cache_keys.shape[2] // heads
    half = width // 2
    length = cache_keys.shape[1]
    scale = half ** (-0.5)

    def project(weight, size):
        return (
            jnp.dot(normed, weight, preferred_element_type=jnp.float32)
            .astype(jnp.bfloat16)
            .reshape(seqs, heads, size)
        )

    q_first = project(q_first_w, half)
    q_second = project(q_second_w, half)
    k_first = project(k_first_w, half)
    k_second = project(k_second_w, half)
    new_value = project(value_w, width)
    blank = jnp.zeros_like(q_first)
    queries = jnp.stack(
        [jnp.concatenate([q_first, blank], axis=-1), jnp.concatenate([blank, q_second], axis=-1)],
        axis=2,
    )
    own_keys = jnp.concatenate([k_first, k_second], axis=-1)
    keys = cache_keys.reshape(seqs, length, heads, width)
    values = cache_values.reshape(seqs, length, heads, width)
    scores = (
        jnp.einsum("shpd,sthd->shpt", queries, keys, preferred_element_type=jnp.float32) * scale
    )
    own = jnp.einsum("shpd,shd->shp", queries, own_keys, preferred_element_type=jnp.float32) * scale
    valid = jnp.arange(length, dtype=jnp.int32)[None, :] < lengths[:, None]
    scores = jnp.where(valid[:, None, None, :], scores, -jnp.inf)
    top = jnp.maximum(jnp.max(scores, axis=-1), own)
    raised = jnp.exp(scores - top[..., None])
    own_raised = jnp.exp(own - top)
    total = jnp.sum(raised, axis=-1) + own_raised
    probs = raised / total[..., None]
    own_probs = own_raised / total
    lam = mix_lambda[None, :]
    mixed_w = (probs[:, :, 0] - lam[..., None] * probs[:, :, 1]).astype(jnp.bfloat16)
    own_w = (own_probs[:, :, 0] - lam * own_probs[:, :, 1]).astype(jnp.bfloat16)
    head_out = jnp.einsum("sht,sthd->shd", mixed_w, values, preferred_element_type=jnp.float32)
    head_out = head_out + own_w.astype(jnp.float32)[..., None] * new_value.astype(jnp.float32)
    return rms_scale(head_out, head_gain).astype(jnp.bfloat16).reshape(seqs, heads * width)


def run_experts(buffer, gate_w, up_w, down_w):
    gate = jnp.einsum("bjcd,jdf->bjcf", buffer, gate_w, preferred_element_type=jnp.float32)
    up = jnp.einsum("bjcd,jdf->bjcf", buffer, up_w, preferred_element_type=jnp.float32)
    bound_gate = jnp.minimum(gate, LIMIT)
    bound_up = jnp.clip(up, -LIMIT, LIMIT)
    hidden = ((bound_up + 1.0) * bound_gate * jax.nn.sigmoid(ALPHA * bound_gate)).astype(
        jnp.bfloat16
    )
    total = jnp.einsum(
        "bjcf,jfd->bjcd",
        gathered_copies(hidden, "tp", 3),
        down_w,
        preferred_element_type=jnp.float32,
    )
    return total.astype(jnp.bfloat16)


def per_device(
    tokens,
    lengths,
    cache_keys,
    cache_values,
    attn_gain,
    q_first_w,
    q_second_w,
    k_first_w,
    k_second_w,
    value_w,
    mix_lambda,
    head_gain,
    out_w,
    ffn_gain,
    routes,
    route_logits,
    gate_w,
    up_w,
    down_w,
):
    wide = tokens.astype(jnp.float32)
    normed = rms_scale(wide, attn_gain).astype(jnp.bfloat16)
    attended = attend_heads(
        normed,
        lengths,
        cache_keys,
        cache_values,
        q_first_w,
        q_second_w,
        k_first_w,
        k_second_w,
        value_w,
        mix_lambda,
        head_gain,
    )
    partial_value = jnp.dot(attended, out_w, preferred_element_type=jnp.float32)
    columns = wide.shape[1] // lax.axis_size("tp")
    start = lax.axis_index("tp") * columns
    share = summed_on_arrival(partial_value.astype(jnp.bfloat16), "tp", 1)
    kept = lax.dynamic_slice_in_dim(wide, start, columns, 1) + share
    squares = over_copies(jnp.sum(kept * kept, axis=1), "tp")
    gain_cols = lax.dynamic_slice_in_dim(ffn_gain, start, columns, 0)
    local_in = (kept * lax.rsqrt(squares / wide.shape[1] + EPS)[:, None] * gain_cols).astype(
        jnp.bfloat16
    )
    weights = jax.nn.softmax(route_logits, axis=-1)
    groups = lax.axis_size("ep")
    owned = gate_w.shape[0]
    seqs, top = routes.shape
    capacity = max(2, 2 * seqs * top // (owned * groups))
    expert_ids = jnp.arange(owned * groups, dtype=jnp.int32)
    dispatch, combine = slot_tables(routes[None], weights[None], expert_ids, capacity)
    buffer = jnp.einsum(
        "bsjc,bsd->bjcd",
        dispatch.astype(jnp.bfloat16),
        gathered_copies(local_in, "tp", 1)[None],
        preferred_element_type=jnp.float32,
    ).astype(jnp.bfloat16)
    buffer = buffer.reshape(groups, owned, capacity, -1)
    arrived = lax.all_to_all(buffer, "ep", split_axis=0, concat_axis=0, tiled=True)
    results = run_experts(arrived, gate_w, up_w, down_w)
    returned = lax.all_to_all(results, "ep", split_axis=0, concat_axis=0, tiled=True).reshape(
        1, groups * owned, capacity, -1
    )
    moe = jnp.einsum(
        "bsjc,bjcd->bsd", combine, returned.astype(jnp.float32), precision=lax.Precision.HIGHEST
    )[0]
    return (kept + moe).astype(jnp.bfloat16)


def solution(mesh):
    return jax.shard_map(
        per_device,
        mesh=mesh,
        in_specs=(
            P("ep", None),
            P("ep"),
            P("ep", None, "tp"),
            P("ep", None, "tp"),
            P(),
            P(None, "tp"),
            P(None, "tp"),
            P(None, "tp"),
            P(None, "tp"),
            P(None, "tp"),
            P("tp"),
            P(),
            P("tp", None),
            P(),
            P("ep", None),
            P("ep", None),
            P("ep", None, "tp"),
            P("ep", None, "tp"),
            P("ep", None, "tp"),
        ),
        out_specs=P("ep", "tp"),
        check_vma=False,
    )
```

profile of v0, /device:TPU:0, one launch (start us, length us, event | category | flops | bytes accessed | tf_op | source)
XLA Modules:
  0.0 104.6 jit_solution(9312646912286105611)
XLA Ops:
  0.8 1.0 multiply_reduce_fusion
  1.9 1.3 %fusion.40 = bf16[32,1,64]{2,0,1:T(8,128)(2,1)S(1)} fusion(bf16[2048,64]{0,1:T(8,128)(2,1)} %param.25, f32[2048]{0:T(1024)} %param.23, f32[32]{0:T(128)S(1)} %add_rsqrt_fusion.2, bf16[32,2048]{1,0:T(8,128)(2,1)} %param.19), kind=kOutput, calls=%fused_computation.31 | convolution fusion | flops 8652800 | bytes 405632 | tf_op jit(solution)/shard_map/dot_general | solution.py:85
  3.2 1.3 %fusion.41 = bf16[32,1,64]{2,0,1:T(8,128)(2,1)S(1)} fusion(bf16[2048,64]{0,1:T(8,128)(2,1)} %param.26, f32[2048]{0:T(1024)} %param.23, f32[32]{0:T(128)S(1)} %add_rsqrt_fusion.2, bf16[32,2048]{1,0:T(8,128)(2,1)} %param.19), kind=kOutput, calls=%fused_computation.32 | convolution fusion | flops 8652800 | bytes 405632 | tf_op jit(solution)/shard_map/dot_general | solution.py:85
  4.5 1.3 %fusion.42 = bf16[32,1,64]{2,0,1:T(8,128)(2,1)S(1)} fusion(bf16[2048,64]{0,1:T(8,128)(2,1)} %param.27, f32[2048]{0:T(1024)} %param.23, f32[32]{0:T(128)S(1)} %add_rsqrt_fusion.2, bf16[32,2048]{1,0:T(8,128)(2,1)} %param.19), kind=kOutput, calls=%fused_computation.33 | convolution fusion | flops 8652800 | bytes 405632 | tf_op jit(solution)/shard_map/dot_general | solution.py:85
  5.8 1.3 %fusion.39 = bf16[32,1,64]{2,0,1:T(8,128)(2,1)S(1)} fusion(bf16[2048,64]{0,1:T(8,128)(2,1)} %param.24, f32[2048]{0:T(1024)} %param.23, f32[32]{0:T(128)S(1)} %add_rsqrt_fusion.2, bf16[32,2048]{1,0:T(8,128)(2,1)} %param.19), kind=kOutput, calls=%fused_computation.30 | convolution fusion | flops 8652800 | bytes 405632 | tf_op jit(solution)/shard_map/dot_general | solution.py:85
  7.1 0.8 iota_compare_fusion
  8.2 5.8 %fusion.69 = (f32[32,2]{1,0:T(8,128)S(1)}, f32[32,2,1024]{2,1,0:T(2,128)S(1)}) fusion(bf16[32,1024,128]{2,1,0:T(8,128)(2,1)} %param.21, bf16[32,2,128]{2,0,1:T(8,128)(2,1)S(1)} %maximum_bitcast_fusion, pred[32,1024]{1,0:T(8,128)(4,1)S(1)} %iota_compare_fusion), kind=kOutput, calls=%fused_computation.89 | convolution fusion | flops 16973760 | bytes 8700160 | tf_op jit(solution)/shard_map/shpd,sthd->shpt/dot_general | solution.py:104
  14.7 4.7 %fusion.51 = f32[32,1,128]{2,1,0:T(1,128)S(1)} fusion(bf16[32,1024,128]{2,1,0:T(8,128)(2,1)} %param.22, f32[32,1,2,1024]{3,2,0,1:T(2,128)S(1)} %divide_bitcast_fusion, f32[]{:T(128)} %bitcast.104), kind=kOutput, calls=%fused_computation.51 | convolution fusion | flops 8486912 | bytes 8667140 | tf_op jit(solution)/shard_map/sht,sthd->shd/dot_general | solution.py:118
  20.1 0.7 copy.103
  20.7 4.6 %all-to-all-start = ((bf16[8,32,256]{2,1,0:T(8,128)(2,1)}), bf16[8,32,256]{2,1,0:T(8,128)(2,1)S(1)}, u32[]{:S(2)}, u32[]{:S(2)}) async-start(bf16[8,32,256]{2,1,0:T(8,128)(2,1)} %bitcast.103), calls=%async_computation | async-start | bytes 262144 | tf_op jit(solution)/shard_map/all_to_all | solution.py:35
  26.1 5.3 %all-to-all-done = bf16[8,32,256]{2,1,0:T(8,128)(2,1)S(1)} async-done(((bf16[8,32,256]{2,1,0:T(8,128)(2,1)}), bf16[8,32,256]{2,1,0:T(8,128)(2,1)S(1)}, u32[]{:S(2)}, u32[]{:S(2)}) %all-to-all-start) | async-done | bytes 131104 | tf_op jit(solution)/shard_map/all_to_all | solution.py:35
  32.2 3.3 %all-to-all-start.1 = ((f32[8,1,32]{2,1,0:T(1,128)}), f32[8,1,32]{2,1,0:T(1,128)S(1)}, u32[]{:S(2)}, u32[]{:S(2)}) async-start(f32[8,1,32]{2,1,0:T(1,128)} %broadcast_in_dim.20), calls=%async_computation.1 | async-start | bytes 8192 | tf_op jit(solution)/shard_map/all_to_all | solution.py:13
  35.5 0.8 dynamic_slice.7
  36.3 4.4 %all-to-all-done.1 = f32[8,1,32]{2,1,0:T(1,128)S(1)} async-done(((f32[8,1,32]{2,1,0:T(1,128)}), f32[8,1,32]{2,1,0:T(1,128)S(1)}, u32[]{:S(2)}, u32[]{:S(2)}) %all-to-all-start.1) | async-done | bytes 1056 | tf_op jit(solution)/shard_map/all_to_all | solution.py:13
  41.4 3.4 %all-to-all-start.2 = ((bf16[8,32,256]{2,1,0:T(8,128)(2,1)}), bf16[8,32,256]{2,1,0:T(8,128)(2,1)S(1)}, u32[]{:S(2)}, u32[]{:S(2)}) async-start(bf16[8,32,256]{2,1,0:T(8,128)(2,1)} %broadcast_in_dim.21), calls=%async_computation.2 | async-start | bytes 262144 | tf_op jit(solution)/shard_map/all_to_all | solution.py:13
  44.9 5.9 %all-to-all-done.2 = bf16[8,32,256]{2,1,0:T(8,128)(2,1)S(1)} async-done(((bf16[8,32,256]{2,1,0:T(8,128)(2,1)}), bf16[8,32,256]{2,1,0:T(8,128)(2,1)S(1)}, u32[]{:S(2)}, u32[]{:S(2)}) %all-to-all-start.2) | async-done | bytes 131104 | tf_op jit(solution)/shard_map/all_to_all | solution.py:13
  51.4 0.8 copy.81
  52.2 24.6 %all_to_all.31 = bf16[16,4,4,2048]{3,2,1,0:T(4,128)(2,1)S(1)} all-to-all(bf16[16,4,4,2048]{3,2,1,0:T(4,128)(2,1)S(1)} %bitcast.106), channel_id=1, replica_groups=mesh['ep'=16,'tp'=8] {'ep'}, dimensions={0} | all-to-all | bytes 2097152 | tf_op jit(solution)/shard_map/all_to_all | solution.py:200
  76.9 0.8 fusion.25
  77.7 0.7 copy-done.9
  78.5 0.9 fusion.31
  79.5 12.8 %all_to_all.32 = bf16[8,16,4,4,128]{4,1,3,2,0:T(8,128)(2,1)S(1)} all-to-all(bf16[8,16,4,4,128]{4,1,3,2,0:T(8,128)(2,1)S(1)} %broadcast_in_dim.22), channel_id=1, replica_groups=mesh['ep'=16,'tp'=8] {'tp'}, dimensions={0} | all-to-all | bytes 1048576 | tf_op jit(solution)/shard_map/all_to_all | solution.py:13
  92.8 10.9 %all_to_all.33 = bf16[16,4,4,256]{3,2,1,0:T(4,128)(2,1)S(1)} all-to-all(bf16[16,4,4,256]{3,2,1,0:T(4,128)(2,1)S(1)} %copy.72), channel_id=1, replica_groups=mesh['ep'=16,'tp'=8] {'ep'}, dimensions={0} | all-to-all | bytes 262144 | tf_op jit(solution)/shard_map/all_to_all | solution.py:202
  103.7 0.8 fusion.35
  (58 shorter events, 5.4 us)
Async XLA Ops:
  0.0 92.2 %copy-start = (bf16[4,1024,256]{2,1,0:T(8,128)(2,1)S(1)}, bf16[4,1024,256]{2,1,0:T(8,128)(2,1)}, u32[]{:S(2)}) copy-start(bf16[4,1024,256]{2,1,0:T(8,128)(2,1)} %param.37) | copy-start | bytes 6291460
  14.7 4.7 %copy-start.2 = (bf16[32,2048]{1,0:T(8,128)(2,1)S(1)}, bf16[32,2048]{1,0:T(8,128)(2,1)}, u32[]{:S(2)}) copy-start(bf16[32,2048]{1,0:T(8,128)(2,1)} %param.19) | copy-start | bytes 393220
  14.7 4.7 %copy-start.3 = (bf16[2048,128]{1,0:T(8,128)(2,1)S(1)}, bf16[2048,128]{1,0:T(8,128)(2,1)}, u32[]{:S(2)}) copy-start(bf16[2048,128]{1,0:T(8,128)(2,1)} %param.28) | copy-start | bytes 1572868
  14.7 4.7 %copy-start.6 = (f32[2048]{0:T(1024)S(1)}, f32[2048]{0:T(1024)}, u32[]{:S(2)}) copy-start(f32[2048]{0:T(1024)} %param.23) | copy-start | bytes 24580
  14.7 5.1 %copy-start.4 = (bf16[128,2048]{1,0:T(8,128)(2,1)S(1)}, bf16[128,2048]{1,0:T(8,128)(2,1)}, u32[]{:S(2)}) copy-start(bf16[128,2048]{1,0:T(8,128)(2,1)} %param.31) | copy-start | bytes 1572868
  14.7 5.1 %copy-start.8 = (f32[128]{0:T(128)S(1)}, f32[128]{0:T(128)}, u32[]{:S(2)}) copy-start(f32[128]{0:T(128)} %param.30) | copy-start | bytes 1540
  14.7 10.6 %copy-start.7 = (s32[32,4]{0,1:T(4,128)S(1)}, s32[32,4]{0,1:T(4,128)}, u32[]{:S(2)}) copy-start(s32[32,4]{0,1:T(4,128)} %param.33) | copy-start | bytes 1540
  19.4 6.2 %copy-start.5 = (f32[32,4]{0,1:T(4,128)S(1)}, f32[32,4]{0,1:T(4,128)}, u32[]{:S(2)}) copy-start(f32[32,4]{0,1:T(4,128)} %param.34) | copy-start | bytes 1540
  20.7 10.7 %all-to-all-start = ((bf16[8,32,256]{2,1,0:T(8,128)(2,1)}), bf16[8,32,256]{2,1,0:T(8,128)(2,1)S(1)}, u32[]{:S(2)}, u32[]{:S(2)}) async-start(bf16[8,32,256]{2,1,0:T(8,128)(2,1)} %bitcast.103), calls=%async_computation | async-start | bytes 262144 | tf_op jit(solution)/shard_map/all_to_all | solution.py:35
  32.2 8.5 %all-to-all-start.1 = ((f32[8,1,32]{2,1,0:T(1,128)}), f32[8,1,32]{2,1,0:T(1,128)S(1)}, u32[]{:S(2)}, u32[]{:S(2)}) async-start(f32[8,1,32]{2,1,0:T(1,128)} %broadcast_in_dim.20), calls=%async_computation.1 | async-start | bytes 8192 | tf_op jit(solution)/shard_map/all_to_all | solution.py:13
  41.4 9.4 %all-to-all-start.2 = ((bf16[8,32,256]{2,1,0:T(8,128)(2,1)}), bf16[8,32,256]{2,1,0:T(8,128)(2,1)S(1)}, u32[]{:S(2)}, u32[]{:S(2)}) async-start(bf16[8,32,256]{2,1,0:T(8,128)(2,1)} %broadcast_in_dim.21), calls=%async_computation.2 | async-start | bytes 262144 | tf_op jit(solution)/shard_map/all_to_all | solution.py:13
  51.4 25.5 %copy-start.1 = (bf16[4,2048,128]{2,1,0:T(8,128)(2,1)S(1)}, bf16[4,2048,128]{2,1,0:T(8,128)(2,1)}, u32[]{:S(2)}) copy-start(bf16[4,2048,128]{2,1,0:T(8,128)(2,1)} %param.35) | copy-start | bytes 6291460
  76.9 1.6 %copy-start.9 = (bf16[4,2048,128]{2,1,0:T(8,128)(2,1)S(1)}, bf16[4,2048,128]{2,1,0:T(8,128)(2,1)}, u32[]{:S(2)}) copy-start(bf16[4,2048,128]{2,1,0:T(8,128)(2,1)} %param.36) | copy-start | bytes 6291460
where the time goes:
time: 105 us
  blocking collectives  48.3 us (46%)
  matrix products  19.9 us (19%)
  waiting for transfers between devices  15.6 us (15%)
  starting transfers between devices  11.3 us (11%)
  local copies, waits for them, and re-layouts  5.14 us (5%)
  other arithmetic  3.3 us (3%)
  between operations  1.09 us (1%)
    all_to_all x1, blocking collectives, per_device(): lax.all_to_all(buffer, 'ep', split_axis=0, concat_axis=0, tiled=True)  24.6 us
    all_to_all x1, blocking collectives, sent_to_all(): return lax.all_to_all(copies, axis, split_axis=0, concat_axis=0, tiled=True)  12.8 us
    all_to_all x1, blocking collectives, per_device(): lax.all_to_all(results, 'ep', split_axis=0, concat_axis=0, tiled=True)  10.9 us
    all_to_all x2, waiting for transfers between devices, sent_to_all(): return lax.all_to_all(copies, axis, split_axis=0, concat_axis=0, tiled=True)  10.2 us
    all_to_all x2, starting transfers between devices, sent_to_all(): return lax.all_to_all(copies, axis, split_axis=0, concat_axis=0, tiled=True)  6.68 us
    dot_general x1, matrix products, attend_heads(): jnp.einsum('shpd,sthd->shpt', queries, keys, preferred_element_type=jnp.f...  5.75 us
    dot_general x5, matrix products, project(): jnp.dot(normed, weight, preferred_element_type=jnp.float32)  5.6 us
    all_to_all x1, waiting for transfers between devices, summed_on_arrival(): lax.all_to_all(parts, axis, split_axis=0, concat_axis=0, tiled=True)  5.34 us
  transfers between devices with their start and end apart: 3, of which 3 were waited for; matrix products, arithmetic and copies ran while one was open for 2% of the time, Pallas kernels for 0%

commit v1 on v0

v1 whole, which is shorter than its diff:
```python
import jax
import jax.numpy as jnp
from jax import lax
from jax.experimental import pallas as pl
from jax.experimental.pallas import tpu as pltpu
from jax.sharding import PartitionSpec as P

EPS = 1e-06
LIMIT = 7.0
ALPHA = 1.702
MESH = pl.DeviceIdType.MESH
F32 = jnp.float32
BF16 = jnp.bfloat16

SMALL = ("tokens", "lengths", "attn_gain", "mix_lambda", "head_gain", "ffn_gain", "routes", "route_logits")
PROJ = ("q_first_w", "q_second_w", "k_first_w", "k_second_w", "value_w")
LATE = ("out_w", "gate_w", "up_w", "down_w")
CHUNKS = 4


def dot(a, b):
    return jnp.dot(a, b, preferred_element_type=F32)


def dot_nt(a, b):
    return lax.dot_general(a, b, (((1,), (1,)), ((), ())), preferred_element_type=F32)


def dot_tn(a, b):
    return lax.dot_general(a, b, (((0,), (0,)), ((), ())), preferred_element_type=F32)


def iota(shape, dim):
    return lax.broadcasted_iota(jnp.int32, shape, dim)


def load_plan(hbm, vm, sems):
    plan = {}
    for name in SMALL + PROJ:
        plan[name] = pltpu.make_async_copy(hbm[name], vm[name], sems.at[len(plan)])
    rows = hbm["cache_keys"].shape[1] // CHUNKS
    seqs = hbm["cache_keys"].shape[0] // CHUNKS
    for i in range(CHUNKS):
        part = pl.ds(i * rows, rows)
        plan["keys", i] = pltpu.make_async_copy(
            hbm["cache_keys"].at[:, part, :], vm["cache_keys"].at[:, part, :], sems.at[len(plan)]
        )
    for i in range(CHUNKS):
        part = pl.ds(i * seqs, seqs)
        plan["values", i] = pltpu.make_async_copy(
            hbm["cache_values"].at[part], vm["cache_values"].at[part], sems.at[len(plan)]
        )
    for name in LATE:
        plan[name] = pltpu.make_async_copy(hbm[name], vm[name], sems.at[len(plan)])
    return plan


N_LOADS = len(SMALL + PROJ + LATE) + 2 * CHUNKS


def attend(plan, vm, qbd, scores, wt, len_row, part_ref):
    for name in ("tokens", "attn_gain", "lengths", "mix_lambda", "head_gain"):
        plan[name].wait()
    seqs, width = vm["tokens"].shape
    length, dim = vm["cache_keys"].shape[1:]
    half = dim // 2
    tok = vm["tokens"][...].astype(F32)
    mean_sq = jnp.mean(tok * tok, axis=1, keepdims=True)
    normed = (tok * lax.rsqrt(mean_sq + EPS) * vm["attn_gain"][...]).astype(BF16)
    len_row[...] = jnp.zeros_like(len_row)
    len_row[0:1, 0:seqs] = vm["lengths"][...]

    def project(name):
        plan[name].wait()
        return dot(normed, vm[name][...]).astype(BF16)

    pad = jnp.zeros((dim - seqs, half), BF16)
    row = iota((dim, half), 0)
    col = iota((dim, half), 1)
    upper = (row == col).astype(F32).astype(BF16)
    lower = (row == col + half).astype(F32).astype(BF16)

    def columns(first, second):
        return dot_nt(upper, jnp.concatenate([first, pad], axis=0)) + dot_nt(
            lower, jnp.concatenate([second, pad], axis=0)
        )

    q_t = columns(project("q_first_w"), project("q_second_w")) * (half ** (-0.5))
    d_row = iota((dim, dim), 0)
    d_col = iota((dim, dim), 1)
    q_a = jnp.where(d_row < half, q_t, 0.0)
    q_b = jnp.where(d_row < half, 0.0, q_t)
    for s in range(seqs):
        mine = d_col == s
        qbd[s * dim : (s + 1) * dim, 0:dim] = jnp.where(mine, q_a, 0.0).astype(BF16)
        qbd[s * dim : (s + 1) * dim, dim : 2 * dim] = jnp.where(mine, q_b, 0.0).astype(BF16)
    k_t = columns(project("k_first_w"), project("k_second_w"))
    own = jnp.concatenate(
        [jnp.sum(q_a * k_t, axis=0, keepdims=True), jnp.sum(q_b * k_t, axis=0, keepdims=True)], axis=1
    )
    new_value = project("value_w").astype(F32)
    len_one = len_row[0:1, :]
    lens = jnp.concatenate([len_one, len_one], axis=1)
    rows = length // CHUNKS
    top = own
    for i in range(CHUNKS):
        plan["keys", i].wait()
        keys = jnp.concatenate(
            [vm["cache_keys"][s, i * rows : (i + 1) * rows, :] for s in range(seqs)], axis=1
        )
        got = dot(keys, qbd[...])
        valid = iota((rows, 2 * dim), 0) + i * rows < lens
        got = jnp.where(valid, got, -jnp.inf)
        scores[i * rows : (i + 1) * rows, :] = got
        top = jnp.maximum(top, jnp.max(got, axis=0, keepdims=True))
    own_raised = jnp.exp(own - top)
    total = own_raised
    for i in range(CHUNKS):
        raised = jnp.exp(scores[i * rows : (i + 1) * rows, :] - top)
        scores[i * rows : (i + 1) * rows, :] = raised
        total = total + jnp.sum(raised, axis=0, keepdims=True)
    inverse = 1.0 / total
    first = inverse[:, 0:dim]
    second = inverse[:, dim : 2 * dim] * vm["mix_lambda"][...]
    for i in range(length // dim):
        block = scores[i * dim : (i + 1) * dim, :]
        mixed = block[:, 0:dim] * first - block[:, dim : 2 * dim] * second
        wt[:, i * dim : (i + 1) * dim] = mixed.T[0:seqs, :].astype(BF16)
    own_w = own_raised[:, 0:dim] * first - own_raised[:, dim : 2 * dim] * second
    own_col = jnp.broadcast_to(own_w, (dim, dim)).T[0:seqs, :].astype(BF16).astype(F32)
    group = 16
    place = iota((group, dim), 0)
    outs = [jnp.zeros((group, dim), F32) for _ in range(seqs // group)]
    per = seqs // CHUNKS
    for i in range(CHUNKS):
        plan["values", i].wait()
        for s in range(i * per, (i + 1) * per, 2):
            g = s // group
            both = jnp.concatenate([vm["cache_values"][s], vm["cache_values"][s + 1]], axis=1)
            got = dot(wt[g * group : (g + 1) * group, :], both)
            outs[g] = outs[g] + jnp.where(place == s % group, got[:, 0:dim], 0.0)
            outs[g] = outs[g] + jnp.where(place == s % group + 1, got[:, dim : 2 * dim], 0.0)
    head_out = jnp.concatenate(outs, axis=0) + own_col * new_value
    mean_sq = jnp.mean(head_out * head_out, axis=1, keepdims=True)
    attended = (head_out * lax.rsqrt(mean_sq + EPS) * vm["head_gain"][...]).astype(BF16)
    plan["out_w"].wait()
    blocks, _, cols = part_ref.shape
    for b in range(blocks):
        part_ref[b] = dot(attended, vm["out_w"][:, b * cols : (b + 1) * cols]).astype(BF16)


def remote(src, dst, send, recv, ep, tp):
    return pltpu.make_async_remote_copy(
        src_ref=src, dst_ref=dst, send_sem=send, recv_sem=recv, device_id=(ep, tp), device_id_type=MESH
    )


def exchange(sizes, plan, vm, bufs, sems, out_ref):
    n_ep, n_tp, owned = sizes
    n_y = n_tp // 2
    e, t = lax.axis_index("ep"), lax.axis_index("tp")
    y, c = t // 2, t % 2
    partner = t + 1 - 2 * c
    part, rs, x1, x2, p1, p2, a1, a2, h2, hid, ret, fin = (bufs[k] for k in BUFS)
    seqs, cols = part.shape[1:]
    hc = cols // 2
    slots = n_ep * 16
    sent = []

    def send(*args):
        copy = remote(*args)
        copy.start()
        sent.append(copy)

    def arrive(buf, sem):
        remote(buf, buf, sems["idle"].at[0], sem, e, partner).wait_recv()

    for k in range(1, n_tp):
        to = (t + k) % n_tp
        send(part.at[to], rs.at[t], sems["rs_s"].at[k], sems["rs_r"].at[t], e, to)
    for name in ("routes", "route_logits", "ffn_gain"):
        plan[name].wait()
    routes, logits = vm["routes"][...], vm["route_logits"][...]
    logits = jnp.exp(logits - jnp.max(logits, axis=1, keepdims=True))
    weights = logits / jnp.sum(logits, axis=1, keepdims=True)
    slot = iota((seqs, slots), 1)
    named = jnp.zeros((seqs, slots), F32)
    weight = jnp.zeros((seqs, slots), F32)
    for k in range(routes.shape[1]):
        hit = routes[:, k : k + 1] == slot // 4
        named = jnp.where(hit, 1.0, named)
        weight = jnp.where(hit, weights[:, k : k + 1], weight)
    before = (iota((seqs, seqs), 1) < iota((seqs, seqs), 0)).astype(F32).astype(BF16)
    rank = dot(before, named.astype(BF16))
    taken = (named > 0.5) & (rank == (slot % 4).astype(F32))
    dispatch = jnp.where(taken, 1.0, 0.0).astype(BF16)
    combine = jnp.where(taken, weight, 0.0)
    combine_hi = combine.astype(BF16)
    combine_lo = (combine - combine_hi.astype(F32)).astype(BF16)
    start = pl.multiple_of(t * cols, cols)
    kept = vm["tokens"][:, pl.ds(start, cols)].astype(F32) + part[t].astype(F32)
    gain = vm["ffn_gain"][:, pl.ds(start, cols)]
    for k in range(1, n_tp):
        frm = (t + k) % n_tp
        arrive(rs.at[frm], sems["rs_r"].at[frm])
        kept = kept + rs[frm].astype(F32)
    ready = (kept * gain).astype(BF16)

    h2[y] = ready[:, hc:]
    for k in range(1, n_y):
        to = (t + 2 * k) % n_tp
        send(h2.at[y], h2.at[y], sems["h2_s"].at[k], sems["h2_r"].at[y], e, to)
    a1[...] = dot_tn(dispatch, ready[:, :hc]).astype(BF16).reshape(a1.shape)
    for k in range(1, n_ep):
        to = (e + k) % n_ep
        send(a1.at[to], x1.at[y, e], sems["x1_s"].at[k], sems["x1_r"].at[e], to, t)
    x1[y, e] = a1[e]
    for k in range(1, n_y):
        frm = (y + k) % n_y
        arrive(h2.at[frm], sems["h2_r"].at[frm])
    second = jnp.concatenate([h2[i] for i in range(n_y)], axis=1)
    a2[...] = dot_tn(dispatch, second).astype(BF16).reshape(a2.shape)
    for k in range(1, n_ep):
        to = (e + k) % n_ep
        send(a2.at[to], x2.at[e], sems["x2_s"].at[k], sems["x2_r"].at[e], to, t)
    x2[e] = a2[e]
    send(a2.at[e], p2.at[e], sems["d2_s"].at[0], sems["d2_r"].at[e], e, partner)
    for k in range(1, n_ep):
        frm = (e + k) % n_ep
        arrive(x1.at[y, frm], sems["x1_r"].at[frm])
    for k in range(1, n_y):
        to = (t + 2 * k) % n_tp
        send(x1.at[y], x1.at[y], sems["y1_s"].at[k], sems["y1_r"].at[y], e, to)
    send(x1.at[y], p1.at[y], sems["d1_s"].at[0], sems["d1_r"].at[y], e, partner)
    for k in range(1, n_y):
        frm = (y + k) % n_y
        arrive(x1.at[frm], sems["y1_r"].at[frm])
        send(x1.at[frm], p1.at[frm], sems["d1_s"].at[k], sems["d1_r"].at[frm], e, partner)
    for k in range(1, n_ep):
        frm = (e + n_ep - k) % n_ep
        arrive(x2.at[frm], sems["x2_r"].at[frm])
        send(x2.at[frm], p2.at[frm], sems["d2_s"].at[k], sems["d2_r"].at[frm], e, partner)

    for name in ("gate_w", "up_w", "down_w"):
        plan[name].wait()
    expert = iota((slots, 2 * vm["gate_w"].shape[2]), 0) % 16 // 4
    squares = jnp.zeros((slots, hc), F32)
    both = jnp.zeros(expert.shape, F32)
    back = 1.0 / vm["ffn_gain"][...]
    bufs["back"][...] = back * back
    for one, two, core in ((x1, x2, c), (p1, p2, 1 - c)):
        if one is p1:
            for i in range(n_y):
                arrive(p1.at[i], sems["d1_r"].at[i])
            for i in range(n_ep):
                arrive(p2.at[i], sems["d2_r"].at[i])
        spread = two[...].reshape(slots, n_y * hc)
        tiles, begins = [], []
        for i in range(n_y):
            begin = pl.multiple_of((2 * i + core) * cols, cols)
            begins.append(begin)
            a = one[i].reshape(slots, hc)
            b = spread[:, i * hc : (i + 1) * hc]
            tiles += [a, b]
            back_sq = bufs["back"][:, pl.ds(begin, cols)]
            squares = squares + a.astype(F32) * a.astype(F32) * back_sq[:, :hc]
            squares = squares + b.astype(F32) * b.astype(F32) * back_sq[:, hc:]
        rows_in = jnp.concatenate(tiles, axis=1)
        for j in range(owned):
            gates = jnp.concatenate([vm["gate_w"][j, pl.ds(b, cols), :] for b in begins], axis=0)
            ups = jnp.concatenate([vm["up_w"][j, pl.ds(b, cols), :] for b in begins], axis=0)
            got = dot(rows_in, jnp.concatenate([gates, ups], axis=1))
            both = both + jnp.where(expert == j, got, 0.0)
    scale = lax.rsqrt(jnp.sum(squares, axis=1, keepdims=True) / (n_tp * cols) + EPS)
    both = both * scale
    ff = vm["gate_w"].shape[2]
    gate = jnp.minimum(both[:, :ff], LIMIT)
    up = jnp.clip(both[:, ff:], -LIMIT, LIMIT)
    hid[t] = ((up + 1.0) * gate / (1.0 + jnp.exp(-ALPHA * gate))).astype(BF16)

    for k in range(1, n_y):
        to = (t + 2 * k) % n_tp
        send(hid.at[t], hid.at[t], sems["hy_s"].at[k], sems["hy_r"].at[y], e, to)
    send(hid.at[t], hid.at[t], sems["hd_s"].at[0], sems["hd_r"].at[y], e, partner)
    for k in range(1, n_y):
        frm = (y + k) % n_y
        block = hid.at[2 * frm + c]
        arrive(block, sems["hy_r"].at[frm])
        send(block, block, sems["hd_s"].at[k], sems["hd_r"].at[frm], e, partner)
    for i in range(n_y):
        arrive(hid.at[2 * i + 1 - c], sems["hd_r"].at[i])
    hidden = jnp.concatenate([hid[i] for i in range(n_tp)], axis=1)
    expert = iota((slots, cols), 0) % 16 // 4
    result = jnp.zeros((slots, cols), F32)
    for j in range(owned):
        result = result + jnp.where(expert == j, dot(hidden, vm["down_w"][j]), 0.0)
    ret[...] = result.astype(BF16).reshape(ret.shape)

    for k in range(1, n_ep):
        to = (e + k) % n_ep
        send(ret.at[to], fin.at[e], sems["re_s"].at[k], sems["re_r"].at[e], to, t)
    fin[e] = ret[e]
    for k in range(1, n_ep):
        frm = (e + n_ep - k) % n_ep
        arrive(fin.at[frm], sems["re_r"].at[frm])
    back_rows = fin[...].reshape(slots, cols)
    moe = dot(combine_hi, back_rows) + dot(combine_lo, back_rows)
    out_ref[...] = kept + moe
    for copy in sent:
        copy.wait_send()


BUFS = ("part", "rs", "x1", "x2", "p1", "p2", "a1", "a2", "h2", "hid", "ret", "fin")


def buffers(n_ep, n_tp, seqs, cols, ff):
    n_y, hc, slots = n_tp // 2, cols // 2, n_ep * 16
    v = lambda *shape: pltpu.VMEM(shape, BF16)
    return {
        "part": v(n_tp, seqs, cols),
        "rs": v(n_tp, seqs, cols),
        "x1": v(n_y, n_ep, 16, hc),
        "x2": v(n_ep, 16, n_y * hc),
        "p1": v(n_y, n_ep, 16, hc),
        "p2": v(n_ep, 16, n_y * hc),
        "a1": v(n_ep, 16, hc),
        "a2": v(n_ep, 16, n_y * hc),
        "h2": v(n_y, seqs, hc),
        "hid": v(n_tp, slots, ff),
        "ret": v(n_ep, 16, cols),
        "fin": v(n_ep, 16, cols),
        "back": pltpu.VMEM((1, n_tp * cols), F32),
    }


def semaphores(n_ep, n_tp):
    n_y = n_tp // 2
    d = lambda n: pltpu.SemaphoreType.DMA((n,))
    return {
        "idle": d(1),
        "rs_s": d(n_tp), "rs_r": d(n_tp),
        "h2_s": d(n_y), "h2_r": d(n_y),
        "x1_s": d(n_ep), "x1_r": d(n_ep),
        "x2_s": d(n_ep), "x2_r": d(n_ep),
        "y1_s": d(n_y), "y1_r": d(n_y),
        "d1_s": d(n_y), "d1_r": d(n_y),
        "d2_s": d(n_ep), "d2_r": d(n_ep),
        "hy_s": d(n_y), "hy_r": d(n_y),
        "hd_s": d(n_y), "hd_r": d(n_y),
        "re_s": d(n_ep), "re_r": d(n_ep),
    }


NAMES = (
    "tokens", "lengths", "cache_keys", "cache_values", "attn_gain", "q_first_w", "q_second_w", "k_first_w",
    "k_second_w", "value_w", "mix_lambda", "head_gain", "out_w", "ffn_gain", "routes", "route_logits",
    "gate_w", "up_w", "down_w",
)


def kernel_of(sizes, with_exchange=True):
    n_ep, n_tp, _ = sizes

    def kernel(hbm, out_ref, vm, attn_bufs, bufs, sems, load_sems):
        plan = load_plan(hbm, vm, load_sems)
        for copy in plan.values():
            copy.start()
        if with_exchange:
            e, t = lax.axis_index("ep"), lax.axis_index("tp")
            barrier = pltpu.get_barrier_semaphore()
            for k in range(1, n_tp):
                pl.semaphore_signal(barrier, inc=1, device_id=(e, (t + k) % n_tp), device_id_type=MESH)
            for k in range(1, n_ep):
                pl.semaphore_signal(barrier, inc=1, device_id=((e + k) % n_ep, t), device_id_type=MESH)
        attend(plan, vm, *attn_bufs, bufs["part"])
        if with_exchange:
            pl.semaphore_wait(barrier, n_tp + n_ep - 2)
            exchange(sizes, plan, vm, bufs, sems, out_ref)
        else:
            for name in ("routes", "route_logits", "ffn_gain", "gate_w", "up_w", "down_w"):
                plan[name].wait()
            for b in range(n_tp):
                out_ref[b] = bufs["part"][b].astype(F32)

    return kernel


def run(n_ep, n_tp, args, with_exchange=True):
    hbm = dict(zip(NAMES, args, strict=True))
    for name in ("lengths", "attn_gain", "mix_lambda", "head_gain", "ffn_gain"):
        hbm[name] = hbm[name].reshape(1, -1)
    seqs, width = hbm["tokens"].shape
    length, dim = hbm["cache_keys"].shape[1:]
    owned, _, ff = hbm["gate_w"].shape
    cols = width // n_tp
    vm = {name: pltpu.VMEM(x.shape, x.dtype) for name, x in hbm.items()}
    attn_bufs = [
        pltpu.VMEM((seqs * dim, 2 * dim), BF16),
        pltpu.VMEM((length, 2 * dim), F32),
        pltpu.VMEM((seqs, length), BF16),
        pltpu.VMEM((8, dim), jnp.int32),
    ]
    out = (seqs, cols) if with_exchange else (n_tp, seqs, cols)
    params = {"collective_id": 0, "has_side_effects": True} if with_exchange else {}
    return pl.pallas_call(
        kernel_of((n_ep, n_tp, owned), with_exchange),
        out_shape=jax.ShapeDtypeStruct(out, F32),
        in_specs=[{name: pl.BlockSpec(memory_space=pl.ANY) for name in hbm}],
        out_specs=pl.BlockSpec(memory_space=pltpu.VMEM),
        scratch_shapes=[
            vm, attn_bufs, buffers(n_ep, n_tp, seqs, cols, ff), semaphores(n_ep, n_tp),
            pltpu.SemaphoreType.DMA((N_LOADS,)),
        ],
        compiler_params=pltpu.CompilerParams(vmem_limit_bytes=56 * 1024 * 1024, **params),
    )(hbm)


def solution(mesh):
    n_ep, n_tp = mesh.shape["ep"], mesh.shape["tp"]

    def per_device(*args):
        return run(n_ep, n_tp, args).astype(BF16)

    return jax.shard_map(
        per_device,
        mesh=mesh,
        in_specs=(
            P("ep", None),
            P("ep"),
            P("ep", None, "tp"),
            P("ep", None, "tp"),
            P(),
            P(None, "tp"),
            P(None, "tp"),
            P(None, "tp"),
            P(None, "tp"),
            P(None, "tp"),
            P("tp"),
            P(),
            P("tp", None),
            P(),
            P("ep", None),
            P("ep", None),
            P("ep", None, "tp"),
            P("ep", None, "tp"),
            P("ep", None, "tp"),
        ),
        out_specs=P("ep", "tp"),
        check_vma=False,
    )
```

time: 105 us -> 57.4 us (0.55)
  blocking collectives: 48.3 us -> 0 us
  Pallas kernels: 0 us -> 45.2 us
  matrix products: 19.9 us -> 0 us
  waiting for transfers between devices: 15.6 us -> 0 us
  starting transfers between devices: 11.3 us -> 0 us
  local copies, waits for them, and re-layouts: 5.14 us -> 9.64 us
  other arithmetic: 3.3 us -> 1.37 us
    all_to_all x3 -> x0, blocking collectives: 48.3 us -> none  [the longest x1 24.6 us: per_device(): lax.all_to_all(buffer, 'ep', split_axis=0, concat_axis=0, tiled=True)]
    pallas_call x0 -> x1, Pallas kernels: none -> 45.2 us  [run(): pl.pallas_call(kernel_of((n_ep, n_tp, owned), with_exchange), out_shape=j...]
    dot_general x14 -> x0, matrix products: 19.9 us -> none  [the longest x1 5.75 us: attend_heads(): jnp.einsum('shpd,sthd->shpt', queries, keys, preferred_element_type=jnp.f...]
    all_to_all x3 -> x0, waiting for transfers between devices: 15.6 us -> none  [the longest x2 10.2 us: sent_to_all(): return lax.all_to_all(copies, axis, split_axis=0, concat_axis=0, tiled=True)]
    all_to_all x3 -> x0, starting transfers between devices: 11.3 us -> none  [the longest x2 6.68 us: sent_to_all(): return lax.all_to_all(copies, axis, split_axis=0, concat_axis=0, tiled=True)]
    unnamed x21 -> x8, local copies, waits for them, and re-layouts: 0.88 us -> 9.64 us
    reduce_sum x8 -> x0, other arithmetic: 1.9 us -> none  [the longest x1 1.04 us: rms_scale(): mean_sq = jnp.mean(rows * rows, axis=-1, keepdims=True)]
    reshape x2 -> x0, local copies, waits for them, and re-layouts: 1.47 us -> none  [the longest x1 0.81 us: per_device(): buffer = buffer.reshape(groups, owned, capacity, -1)]
  transfers between devices with their start and end apart: 3 -> 0, of which waited for: 3 -> 0; matrix products, arithmetic and copies ran while one was open for 2% -> 0% of each run, Pallas kernels for 0% -> 0%
where the time goes in v1:
time: 57.4 us; the launch traced here: 56.9 us
  Pallas kernels  45.2 us (79%)
  local copies, waits for them, and re-layouts  9.64 us (17%)
  other arithmetic  1.37 us (2%)
  between operations  0.71 us (1%)
    pallas_call x1, Pallas kernels, run(): pl.pallas_call(kernel_of((n_ep, n_tp, owned), with_exchange), out_shape=j...  45.2 us
    unnamed x8, local copies, waits for them, and re-layouts  9.64 us
    convert_element_type x1, other arithmetic, per_device(): return run(n_ep, n_tp, args).astype(BF16)  1.37 us

profile of v1, /device:TPU:0, one launch (start us, length us, event | category | flops | bytes accessed | tf_op | source)
XLA Modules:
  0.0 56.9 jit_solution(14322494831898715891)
XLA Ops:
  0.0 0.0 copy-start
  0.7 1.4 %copy.25.hbm__routes__ = s32[32,4]{1,0:T(8,128)} copy(s32[32,4]{0,1:T(4,128)} %param.33) | data formatting | bytes 1024 | tf_op args[14]
  2.1 1.4 %copy.24.hbm__route_logits__ = f32[32,4]{1,0:T(8,128)} copy(f32[32,4]{0,1:T(4,128)} %param.34) | data formatting | bytes 1024 | tf_op args[15]
  3.4 2.0 %copy.22.hbm__q_first_w__ = bf16[2048,64]{1,0:T(8,128)(2,1)} copy(bf16[2048,64]{0,1:T(8,128)(2,1)} %param.24) | data formatting | bytes 524288 | tf_op args[5]
  5.4 2.0 %copy.23.hbm__q_second_w__ = bf16[2048,64]{1,0:T(8,128)(2,1)} copy(bf16[2048,64]{0,1:T(8,128)(2,1)} %param.25) | data formatting | bytes 524288 | tf_op args[6]
  7.4 1.9 %copy.20.hbm__k_first_w__ = bf16[2048,64]{1,0:T(8,128)(2,1)} copy(bf16[2048,64]{0,1:T(8,128)(2,1)} %param.26) | data formatting | bytes 524288 | tf_op args[7]
  9.3 0.0 copy-done
  9.3 1.0 %copy.21.hbm__k_second_w__ = bf16[2048,64]{1,0:T(8,128)(2,1)} copy(bf16[2048,64]{0,1:T(8,128)(2,1)S(1)} %copy-done) | data formatting | bytes 524288 | tf_op args[8]
  10.3 45.2 %shard_map.181 = f32[32,256]{1,0:T(8,128)} custom-call(f32[1,2048]{1,0:T(1,128)} %bitcast.6, bf16[32,1024,128]{2,1,0:T(8,128)(2,1)} %hbm__cache_keys__.1, bf16[32,1024,128]{2,1,0:T(8,128)(2,1)} %hbm__cache_values__.1, bf16[4,1024,256]{2,1,0:T(8,128)(2,1)} %hbm__down_w__.1, f32[1,2048]{1,0:T(1,128)} %bitcast.7, bf16[4,2048,128]{2,1,0:T(8,128)(2,1)} %hbm__gate_w__.1, ...), custom_call_target="tpu_custom_call" | custom-call | tf_op jit(solution)/shard_map/pallas_call | solution.py:405
  55.6 1.4 %convert_element_type.3 = bf16[32,256]{1,0:T(8,128)(2,1)} convert(f32[32,256]{1,0:T(8,128)} %shard_map.181) | non-fusion elementwise | flops 8192 | bytes 49152 | tf_op jit(solution)/shard_map/convert_element_type | solution.py:422
Async XLA Ops:
  0.0 9.3 %copy-start = (bf16[2048,64]{0,1:T(8,128)(2,1)S(1)}, bf16[2048,64]{0,1:T(8,128)(2,1)}, u32[]{:S(2)}) copy-start(bf16[2048,64]{0,1:T(8,128)(2,1)} %param.27) | copy-start | bytes 786436

commit v2 on v0

v2 whole, which is shorter than its diff:
```python
from typing import Any, NamedTuple

import jax
import jax.numpy as jnp
from jax import lax
from jax.experimental import pallas as pl
from jax.experimental.pallas import tpu as pltpu
from jax.sharding import PartitionSpec as P

EPS = 1e-06
LIMIT = 7.0
ALPHA = 1.702
MESH = pl.DeviceIdType.MESH
F32 = jnp.float32
BF16 = jnp.bfloat16
CHUNKS = 4
ROWS = 16
scope = jax.named_scope


class Args(NamedTuple):
    tokens: Any
    lengths: Any
    cache_keys: Any
    cache_values: Any
    attn_gain: Any
    q_first_w: Any
    q_second_w: Any
    k_first_w: Any
    k_second_w: Any
    value_w: Any
    mix_lambda: Any
    head_gain: Any
    out_w: Any
    ffn_gain: Any
    routes: Any
    route_logits: Any
    gate_w: Any
    up_w: Any
    down_w: Any


class Held(NamedTuple):
    tokens: Any
    lengths: Any
    cache_keys: Any
    cache_values: Any
    attn_gain: Any
    narrow_w: Any
    value_w: Any
    mix_lambda: Any
    head_gain: Any
    out_w: Any
    ffn_gain: Any
    routes: Any
    route_logits: Any
    gate_up_w: Any
    down_w: Any


class Loads(NamedTuple):
    tokens: Any
    attn_gain: Any
    narrow_w: Any
    lengths: Any
    mix_lambda: Any
    head_gain: Any
    value_w: Any
    ffn_gain: Any
    routes: Any
    route_logits: Any
    keys: Any
    values: Any
    out_w: Any
    gate_up_w: Any
    down_w: Any


class Work(NamedTuple):
    queries: Any
    scores: Any
    mixed: Any
    len_row: Any
    narrow: Any


class Bufs(NamedTuple):
    part: Any
    rs: Any
    x1: Any
    x2: Any
    p1: Any
    p2: Any
    a1: Any
    a2: Any
    h2: Any
    hid: Any
    ret: Any
    fin: Any


class Pair(NamedTuple):
    send: Any
    recv: Any


class Sems(NamedTuple):
    idle: Any
    rs: Pair
    h2: Pair
    x1: Pair
    x2: Pair
    y1: Pair
    d1: Pair
    d2: Pair
    hy: Pair
    hd: Pair
    re: Pair


def dot(a, b):
    return jnp.dot(a, b, preferred_element_type=F32)


def dot_nt(a, b):
    return lax.dot_general(a, b, (((1,), (1,)), ((), ())), preferred_element_type=F32)


def iota(shape, dim):
    return lax.broadcasted_iota(jnp.int32, shape, dim)


def plan_loads(hbm, vm, sems):
    count = iter(range(N_LOADS))

    def copy(src, dst):
        return (pltpu.make_async_copy(src, dst, sems.at[next(count)]),)

    half = hbm.q_first_w.shape[0]
    rows = hbm.cache_keys.shape[1] // CHUNKS
    seqs = hbm.cache_keys.shape[0] // CHUNKS
    ff = hbm.gate_w.shape[2]
    narrow = (hbm.q_first_w, hbm.q_second_w, hbm.k_first_w, hbm.k_second_w)
    spans = [pl.ds(i * rows, rows) for i in range(CHUNKS)]
    blocks = [pl.ds(i * seqs, seqs) for i in range(CHUNKS)]
    return Loads(
        tokens=copy(hbm.tokens, vm.tokens),
        attn_gain=copy(hbm.attn_gain, vm.attn_gain),
        narrow_w=sum((copy(w, vm.narrow_w.at[pl.ds(i * half, half)]) for i, w in enumerate(narrow)), ()),
        lengths=copy(hbm.lengths, vm.lengths),
        mix_lambda=copy(hbm.mix_lambda, vm.mix_lambda),
        head_gain=copy(hbm.head_gain, vm.head_gain),
        value_w=copy(hbm.value_w, vm.value_w),
        ffn_gain=copy(hbm.ffn_gain, vm.ffn_gain),
        routes=copy(hbm.routes, vm.routes),
        route_logits=copy(hbm.route_logits, vm.route_logits),
        keys=sum((copy(hbm.cache_keys.at[:, s, :], vm.cache_keys.at[:, s, :]) for s in spans), ()),
        values=sum((copy(hbm.cache_values.at[b], vm.cache_values.at[b]) for b in blocks), ()),
        out_w=copy(hbm.out_w, vm.out_w),
        gate_up_w=copy(hbm.gate_w, vm.gate_up_w.at[:, :, pl.ds(0, ff)])
        + copy(hbm.up_w, vm.gate_up_w.at[:, :, pl.ds(ff, ff)]),
        down_w=copy(hbm.down_w, vm.down_w),
    )


N_LOADS = 17 + 2 * CHUNKS


def wait(copies):
    for copy in copies:
        copy.wait()


def attend(loads, vm, work, part_ref):
    with scope("load"):
        wait(loads.tokens + loads.attn_gain + loads.narrow_w + loads.lengths + loads.mix_lambda)
        wait(loads.head_gain + loads.value_w)
    with scope("proj"):
        seqs, width = vm.tokens.shape
        length, dim = vm.cache_keys.shape[1:]
        half = dim // 2
        tok = vm.tokens[...].astype(F32)
        mean_sq = jnp.mean(tok * tok, axis=1, keepdims=True)
        normed = (tok * lax.rsqrt(mean_sq + EPS) * vm.attn_gain[...]).astype(BF16)
        work.len_row[...] = jnp.zeros_like(work.len_row)
        work.len_row[0:1, 0:seqs] = vm.lengths[...]
        work.narrow[...] = jnp.zeros_like(work.narrow)
        work.narrow[:, 0:seqs] = dot_nt(vm.narrow_w[...], normed).astype(BF16).astype(F32)
        q_t = work.narrow[0:dim, :] * (half ** (-0.5))
        k_t = work.narrow[dim : 2 * dim, :]
        new_value = dot(normed, vm.value_w[...]).astype(BF16).astype(F32)
        d_row = iota((dim, dim), 0)
        d_col = iota((dim, dim), 1)
        q_a = jnp.where(d_row < half, q_t, 0.0)
        q_b = jnp.where(d_row < half, 0.0, q_t)
        for s in range(seqs):
            mine = d_col == s
            work.queries[s * dim : (s + 1) * dim, 0:dim] = jnp.where(mine, q_a, 0.0).astype(BF16)
            work.queries[s * dim : (s + 1) * dim, dim : 2 * dim] = jnp.where(mine, q_b, 0.0).astype(BF16)
        own = jnp.concatenate(
            [jnp.sum(q_a * k_t, axis=0, keepdims=True), jnp.sum(q_b * k_t, axis=0, keepdims=True)], axis=1
        )
        len_one = work.len_row[0:1, :]
        lens = jnp.concatenate([len_one, len_one], axis=1)
    rows = length // CHUNKS
    top = own
    for i in range(CHUNKS):
        with scope("wk"):
            loads.keys[i].wait()
        with scope("qk"):
            keys = jnp.concatenate(
                [vm.cache_keys[s, i * rows : (i + 1) * rows, :] for s in range(seqs)], axis=1
            )
            got = dot(keys, work.queries[...])
            valid = iota((rows, 2 * dim), 0) + i * rows < lens
            got = jnp.where(valid, got, -jnp.inf)
            work.scores[i * rows : (i + 1) * rows, :] = got
            top = jnp.maximum(top, jnp.max(got, axis=0, keepdims=True))
    with scope("soft"):
        own_raised = jnp.exp(own - top)
        total = own_raised
        for i in range(CHUNKS):
            raised = jnp.exp(work.scores[i * rows : (i + 1) * rows, :] - top)
            work.scores[i * rows : (i + 1) * rows, :] = raised
            total = total + jnp.sum(raised, axis=0, keepdims=True)
        inverse = 1.0 / total
        first = inverse[:, 0:dim]
        second = inverse[:, dim : 2 * dim] * vm.mix_lambda[...]
        for i in range(length // dim):
            block = work.scores[i * dim : (i + 1) * dim, :]
            mixed = block[:, 0:dim] * first - block[:, dim : 2 * dim] * second
            work.mixed[:, i * dim : (i + 1) * dim] = mixed.T[0:seqs, :].astype(BF16)
        own_w = own_raised[:, 0:dim] * first - own_raised[:, dim : 2 * dim] * second
        own_col = jnp.broadcast_to(own_w, (dim, dim)).T[0:seqs, :].astype(BF16).astype(F32)
    group = 16
    place = iota((group, dim), 0)
    outs = [jnp.zeros((group, dim), F32) for _ in range(seqs // group)]
    per = seqs // CHUNKS
    for i in range(CHUNKS):
        with scope("wv"):
            loads.values[i].wait()
        with scope("pv"):
            for s in range(i * per, (i + 1) * per, 2):
                g = s // group
                both = jnp.concatenate([vm.cache_values[s], vm.cache_values[s + 1]], axis=1)
                got = dot(work.mixed[g * group : (g + 1) * group, :], both)
                outs[g] = outs[g] + jnp.where(place == s % group, got[:, 0:dim], 0.0)
                outs[g] = outs[g] + jnp.where(place == s % group + 1, got[:, dim : 2 * dim], 0.0)
    with scope("head"):
        head_out = jnp.concatenate(outs, axis=0) + own_col * new_value
        mean_sq = jnp.mean(head_out * head_out, axis=1, keepdims=True)
        attended = (head_out * lax.rsqrt(mean_sq + EPS) * vm.head_gain[...]).astype(BF16)
        wait(loads.out_w)
        blocks, _, cols = part_ref.shape
        for b in range(blocks):
            part_ref[b] = dot(attended, vm.out_w[:, b * cols : (b + 1) * cols]).astype(BF16)


def remote(src, dst, send, recv, ep, tp):
    return pltpu.make_async_remote_copy(
        src_ref=src, dst_ref=dst, send_sem=send, recv_sem=recv, device_id=(ep, tp), device_id_type=MESH
    )


def slot_tables(vm, slots):
    routes, logits = vm.routes[...], vm.route_logits[...]
    top, seqs = routes.shape
    logits = jnp.exp(logits - jnp.max(logits, axis=0, keepdims=True))
    weights = logits / jnp.sum(logits, axis=0, keepdims=True)
    slot = iota((slots, seqs), 0)
    named = jnp.zeros((slots, seqs), F32)
    weight = jnp.zeros((slots, seqs), F32)
    for k in range(top):
        hit = routes[k : k + 1, :] == slot // 4
        named = jnp.where(hit, 1.0, named)
        weight = jnp.where(hit, weights[k : k + 1, :], weight)
    before = (iota((seqs, seqs), 0) < iota((seqs, seqs), 1)).astype(F32).astype(BF16)
    rank = dot(named.astype(BF16), before)
    taken = (named > 0.5) & (rank == (slot % 4).astype(F32))
    return jnp.where(taken, 1.0, 0.0).astype(BF16), jnp.where(taken, weight, 0.0)


def exchange(sizes, loads, vm, bufs, wide, sems, out_ref):
    n_ep, n_tp, owned = sizes
    n_y = n_tp // 2
    e, t = lax.axis_index("ep"), lax.axis_index("tp")
    y, c = t // 2, t % 2
    partner = t + 1 - 2 * c
    part, rs, x1, x2, p1, p2, a1, a2, h2, hid, ret, fin = bufs
    seqs, cols = part.shape[1:]
    hc = cols // 2
    slots = n_ep * ROWS
    sent = []

    def send(src, dst, pair, k, place, ep, tp):
        copy = remote(src, dst, pair.send.at[k], pair.recv.at[place], ep, tp)
        copy.start()
        sent.append(copy)

    def arrive(buf, pair, place):
        remote(buf, buf, sems.idle.at[0], pair.recv.at[place], e, partner).wait_recv()

    with scope("rs"):
        for k in range(1, n_tp):
            to = (t + k) % n_tp
            send(part.at[to], rs.at[t], sems.rs, k, t, e, to)
        wait(loads.routes + loads.route_logits + loads.ffn_gain)
        dispatch, combine = slot_tables(vm, slots)
        wide[...] = jnp.zeros_like(wide)
        wide[:, 0:seqs] = combine
        combine = jnp.concatenate([wide[i : i + 128, :].T[0:seqs, :] for i in range(0, slots, 128)], axis=1)
        combine_hi = combine.astype(BF16)
        combine_lo = (combine - combine_hi.astype(F32)).astype(BF16)
        start = pl.multiple_of(t * cols, cols)
        kept = vm.tokens[:, pl.ds(start, cols)].astype(F32) + part[t].astype(F32)
        gain = vm.ffn_gain[:, pl.ds(start, cols)]
    with scope("rsw"):
        for k in range(1, n_tp):
            frm = (t + k) % n_tp
            arrive(rs.at[frm], sems.rs, frm)
            kept = kept + rs[frm].astype(F32)
        ready = (kept * gain).astype(BF16)

    with scope("d1"):
        h2[y] = ready[:, hc:]
        for k in range(1, n_y):
            to = (t + 2 * k) % n_tp
            send(h2.at[y], h2.at[y], sems.h2, k, y, e, to)
        a1[...] = dot(dispatch, ready[:, :hc]).astype(BF16).reshape(a1.shape)
        for k in range(1, n_ep):
            to = (e + k) % n_ep
            send(a1.at[to], x1.at[y, e], sems.x1, k, e, to, t)
        x1[y, e] = a1[e]
    with scope("h2w"):
        for k in range(1, n_y):
            frm = (y + k) % n_y
            arrive(h2.at[frm], sems.h2, frm)
    with scope("d2"):
        second = jnp.concatenate([h2[i] for i in range(n_y)], axis=1)
        a2[...] = dot(dispatch, second).astype(BF16).reshape(a2.shape)
        for k in range(1, n_ep):
            to = (e + k) % n_ep
            send(a2.at[to], x2.at[e], sems.x2, k, e, to, t)
        x2[e] = a2[e]
        send(a2.at[e], p2.at[e], sems.d2, 0, e, e, partner)
    with scope("x1w"):
        for k in range(1, n_ep):
            frm = (e + k) % n_ep
            arrive(x1.at[y, frm], sems.x1, frm)
        for k in range(1, n_y):
            to = (t + 2 * k) % n_tp
            send(x1.at[y], x1.at[y], sems.y1, k, y, e, to)
        send(x1.at[y], p1.at[y], sems.d1, 0, y, e, partner)
    with scope("y1w"):
        for k in range(1, n_y):
            frm = (y + k) % n_y
            arrive(x1.at[frm], sems.y1, frm)
            send(x1.at[frm], p1.at[frm], sems.d1, k, frm, e, partner)
    with scope("x2w"):
        for k in range(1, n_ep):
            frm = (e + n_ep - k) % n_ep
            arrive(x2.at[frm], sems.x2, frm)
            send(x2.at[frm], p2.at[frm], sems.d2, k, frm, e, partner)

    wait(loads.gate_up_w + loads.down_w)
    ff = vm.gate_up_w.shape[2] // 2
    expert = iota((slots, 2 * ff), 0) % 16 // 4
    squares = jnp.zeros((slots, hc), F32)
    both = jnp.zeros((slots, 2 * ff), F32)
    for one, two, core in ((x1, x2, c), (p1, p2, 1 - c)):
        if one is p1:
            with scope("dw"):
                for i in range(n_y):
                    arrive(p1.at[i], sems.d1, i)
                for i in range(n_ep):
                    arrive(p2.at[i], sems.d2, i)
        with scope("gu"):
            spread = two[...].reshape(slots, n_y * hc)
            tiles, begins = [], []
            for i in range(n_y):
                begin = pl.multiple_of((2 * i + core) * cols, cols)
                begins.append(begin)
                a = one[i].reshape(slots, hc)
                b = spread[:, i * hc : (i + 1) * hc]
                tiles += [a, b]
                back = 1.0 / vm.ffn_gain[:, pl.ds(begin, cols)]
                a, b = a.astype(F32) * back[:, :hc], b.astype(F32) * back[:, hc:]
                squares = squares + a * a + b * b
            rows_in = jnp.concatenate(tiles, axis=1)
            for j in range(owned):
                w = jnp.concatenate([vm.gate_up_w[j, pl.ds(b, cols), :] for b in begins], axis=0)
                both = both + jnp.where(expert == j, dot(rows_in, w), 0.0)
    with scope("act"):
        scale = lax.rsqrt(jnp.sum(squares, axis=1, keepdims=True) / (n_tp * cols) + EPS)
        both = both * scale
        gate = jnp.minimum(both[:, :ff], LIMIT)
        up = jnp.clip(both[:, ff:], -LIMIT, LIMIT)
        hid[t] = ((up + 1.0) * gate / (1.0 + jnp.exp(-ALPHA * gate))).astype(BF16)

        for k in range(1, n_y):
            to = (t + 2 * k) % n_tp
            send(hid.at[t], hid.at[t], sems.hy, k, y, e, to)
        send(hid.at[t], hid.at[t], sems.hd, 0, y, e, partner)
    with scope("hyw"):
        for k in range(1, n_y):
            frm = (y + k) % n_y
            block = hid.at[2 * frm + c]
            arrive(block, sems.hy, frm)
            send(block, block, sems.hd, k, frm, e, partner)
    with scope("hdw"):
        for i in range(n_y):
            arrive(hid.at[2 * i + 1 - c], sems.hd, i)
    with scope("down"):
        hidden = jnp.concatenate([hid[i] for i in range(n_tp)], axis=1)
        expert = iota((slots, cols), 0) % 16 // 4
        result = jnp.zeros((slots, cols), F32)
        for j in range(owned):
            result = result + jnp.where(expert == j, dot(hidden, vm.down_w[j]), 0.0)
        ret[...] = result.astype(BF16).reshape(ret.shape)

        for k in range(1, n_ep):
            to = (e + k) % n_ep
            send(ret.at[to], fin.at[e], sems.re, k, e, to, t)
        fin[e] = ret[e]
    with scope("rew"):
        for k in range(1, n_ep):
            frm = (e + n_ep - k) % n_ep
            arrive(fin.at[frm], sems.re, frm)
    with scope("fin"):
        back_rows = fin[...].reshape(slots, cols)
        moe = dot(combine_hi, back_rows) + dot(combine_lo, back_rows)
        out_ref[...] = (kept + moe).astype(out_ref.dtype)
        for copy in sent:
            copy.wait_send()


def buffers(n_ep, n_tp, seqs, cols, ff):
    n_y, hc = n_tp // 2, cols // 2

    def array(*shape):
        return pltpu.VMEM(shape, BF16)

    return Bufs(
        part=array(n_tp, seqs, cols),
        rs=array(n_tp, seqs, cols),
        x1=array(n_y, n_ep, ROWS, hc),
        x2=array(n_ep, ROWS, n_y * hc),
        p1=array(n_y, n_ep, ROWS, hc),
        p2=array(n_ep, ROWS, n_y * hc),
        a1=array(n_ep, ROWS, hc),
        a2=array(n_ep, ROWS, n_y * hc),
        h2=array(n_y, seqs, hc),
        hid=array(n_tp, n_ep * ROWS, ff),
        ret=array(n_ep, ROWS, cols),
        fin=array(n_ep, ROWS, cols),
    )


def semaphores(n_ep, n_tp):
    n_y = n_tp // 2

    def pair(n):
        return Pair(pltpu.SemaphoreType.DMA((n,)), pltpu.SemaphoreType.DMA((n,)))

    return Sems(
        idle=pltpu.SemaphoreType.DMA((1,)),
        rs=pair(n_tp),
        h2=pair(n_y),
        x1=pair(n_ep),
        x2=pair(n_ep),
        y1=pair(n_y),
        d1=pair(n_y),
        d2=pair(n_ep),
        hy=pair(n_y),
        hd=pair(n_y),
        re=pair(n_ep),
    )


def run(n_ep, n_tp, hbm):
    seqs, width = hbm.tokens.shape
    length, dim = hbm.cache_keys.shape[1:]
    owned, _, ff = hbm.gate_w.shape
    cols = width // n_tp
    hbm = hbm._replace(
        lengths=hbm.lengths.reshape(1, -1),
        attn_gain=hbm.attn_gain.reshape(1, -1),
        head_gain=hbm.head_gain.reshape(1, -1),
        ffn_gain=hbm.ffn_gain.reshape(1, -1),
        mix_lambda=hbm.mix_lambda.reshape(1, -1),
        q_first_w=hbm.q_first_w.T,
        q_second_w=hbm.q_second_w.T,
        k_first_w=hbm.k_first_w.T,
        k_second_w=hbm.k_second_w.T,
        routes=hbm.routes.T,
        route_logits=hbm.route_logits.T,
    )

    def like(x):
        return pltpu.VMEM(x.shape, x.dtype)

    vm = Held(
        tokens=like(hbm.tokens),
        lengths=like(hbm.lengths),
        cache_keys=like(hbm.cache_keys),
        cache_values=like(hbm.cache_values),
        attn_gain=like(hbm.attn_gain),
        narrow_w=pltpu.VMEM((2 * dim, width), BF16),
        value_w=like(hbm.value_w),
        mix_lambda=like(hbm.mix_lambda),
        head_gain=like(hbm.head_gain),
        out_w=like(hbm.out_w),
        ffn_gain=like(hbm.ffn_gain),
        routes=like(hbm.routes),
        route_logits=like(hbm.route_logits),
        gate_up_w=pltpu.VMEM((owned, width, 2 * ff), BF16),
        down_w=like(hbm.down_w),
    )
    work = Work(
        queries=pltpu.VMEM((seqs * dim, 2 * dim), BF16),
        scores=pltpu.VMEM((length, 2 * dim), F32),
        mixed=pltpu.VMEM((seqs, length), BF16),
        len_row=pltpu.VMEM((8, dim), jnp.int32),
        narrow=pltpu.VMEM((2 * dim, dim), F32),
    )

    def kernel(hbm, out_ref, vm, work, bufs, wide, sems, load_sems):
        loads = plan_loads(hbm, vm, load_sems)
        for group in loads:
            for copy in group:
                copy.start()
        e, t = lax.axis_index("ep"), lax.axis_index("tp")
        barrier = pltpu.get_barrier_semaphore()
        for k in range(1, n_tp):
            pl.semaphore_signal(barrier, inc=1, device_id=(e, (t + k) % n_tp), device_id_type=MESH)
        for k in range(1, n_ep):
            pl.semaphore_signal(barrier, inc=1, device_id=((e + k) % n_ep, t), device_id_type=MESH)
        attend(loads, vm, work, bufs.part)
        with scope("bar"):
            pl.semaphore_wait(barrier, n_tp + n_ep - 2)
        exchange((n_ep, n_tp, owned), loads, vm, bufs, wide, sems, out_ref)

    return pl.pallas_call(
        kernel,
        out_shape=jax.ShapeDtypeStruct((seqs, cols), OUT),
        in_specs=[Args(*[pl.BlockSpec(memory_space=pl.ANY)] * len(hbm))],
        out_specs=pl.BlockSpec(memory_space=pltpu.VMEM),
        scratch_shapes=[
            vm,
            work,
            buffers(n_ep, n_tp, seqs, cols, ff),
            pltpu.VMEM((n_ep * ROWS, 128), F32),
            semaphores(n_ep, n_tp),
            pltpu.SemaphoreType.DMA((N_LOADS,)),
        ],
        compiler_params=pltpu.CompilerParams(
            vmem_limit_bytes=56 * 1024 * 1024, collective_id=0, has_side_effects=True
        ),
    )(hbm)


OUT = F32


def solution(mesh):
    n_ep, n_tp = mesh.shape["ep"], mesh.shape["tp"]

    def per_device(*args):
        return run(n_ep, n_tp, Args(*args)).astype(BF16)

    rows, heads, both = P("ep", None), P(None, "tp"), P("ep", None, "tp")
    return jax.shard_map(
        per_device,
        mesh=mesh,
        in_specs=(
            rows, P("ep"), both, both, P(), heads, heads, heads, heads, heads,
            P("tp"), P(), P("tp", None), P(), rows, rows, both, both, both,
        ),
        out_specs=P("ep", "tp"),
        check_vma=False,
    )
```

time: 105 us -> 47.5 us (0.45)
  blocking collectives: 48.3 us -> 0 us
  Pallas kernels: 0 us -> 45.1 us
  matrix products: 19.9 us -> 0 us
  waiting for transfers between devices: 15.6 us -> 0 us
  starting transfers between devices: 11.3 us -> 0 us
  local copies, waits for them, and re-layouts: 5.14 us -> 0 us
  other arithmetic: 3.3 us -> 1.37 us
    all_to_all x3 -> x0, blocking collectives: 48.3 us -> none  [the longest x1 24.6 us: per_device(): lax.all_to_all(buffer, 'ep', split_axis=0, concat_axis=0, tiled=True)]
    pallas_call x0 -> x1, Pallas kernels: none -> 45.1 us  [run(): pl.pallas_call(kernel, out_shape=jax.ShapeDtypeStruct((seqs, cols), OUT),...]
    dot_general x14 -> x0, matrix products: 19.9 us -> none  [the longest x1 5.75 us: attend_heads(): jnp.einsum('shpd,sthd->shpt', queries, keys, preferred_element_type=jnp.f...]
    all_to_all x3 -> x0, waiting for transfers between devices: 15.6 us -> none  [the longest x2 10.2 us: sent_to_all(): return lax.all_to_all(copies, axis, split_axis=0, concat_axis=0, tiled=True)]
    all_to_all x3 -> x0, starting transfers between devices: 11.3 us -> none  [the longest x2 6.68 us: sent_to_all(): return lax.all_to_all(copies, axis, split_axis=0, concat_axis=0, tiled=True)]
    reduce_sum x8 -> x0, other arithmetic: 1.9 us -> none  [the longest x1 1.04 us: rms_scale(): mean_sq = jnp.mean(rows * rows, axis=-1, keepdims=True)]
    reshape x2 -> x0, local copies, waits for them, and re-layouts: 1.47 us -> none  [the longest x1 0.81 us: per_device(): buffer = buffer.reshape(groups, owned, capacity, -1)]
    broadcast_in_dim x3 -> x0, local copies, waits for them, and re-layouts: 1.37 us -> none  [sent_to_all(): copies = jnp.broadcast_to(x, (lax.axis_size(axis), *x.shape))]
  transfers between devices with their start and end apart: 3 -> 0, of which waited for: 3 -> 0; matrix products, arithmetic and copies ran while one was open for 2% -> 0% of each run, Pallas kernels for 0% -> 0%
where the time goes in v2:
time: 47.5 us; the launch traced here: 47.2 us
  Pallas kernels  45.1 us (95%)
  other arithmetic  1.37 us (3%)
  between operations  0.66 us (1%)
    pallas_call x1, Pallas kernels, run(): pl.pallas_call(kernel, out_shape=jax.ShapeDtypeStruct((seqs, cols), OUT),...  45.1 us
    convert_element_type x1, other arithmetic, per_device(): return run(n_ep, n_tp, Args(*args)).astype(BF16)  1.37 us

profile of v2, /device:TPU:0, one launch (start us, length us, event | category | flops | bytes accessed | tf_op | source)
XLA Modules:
  0.0 47.2 jit_solution(13460965486217912786)
XLA Ops:
  0.7 45.1 %shard_map.181 = f32[32,256]{1,0:T(8,128)} custom-call(bf16[32,2048]{1,0:T(8,128)(2,1)} %hbm_tokens.1, s32[1,32]{1,0:T(1,128)} %bitcast.20, bf16[32,1024,128]{2,1,0:T(8,128)(2,1)} %hbm_cache_keys.1, bf16[32,1024,128]{2,1,0:T(8,128)(2,1)} %hbm_cache_values.1, f32[1,2048]{1,0:T(1,128)} %bitcast.16, bf16[64,2048]{1,0:T(8,128)(2,1)} %bitcast.12, ...), custom_call_target="tpu_custom_call" | custom-call | tf_op jit(solution)/shard_map/pallas_call | solution.py:543
  45.8 1.4 %convert_element_type.3 = bf16[32,256]{1,0:T(8,128)(2,1)} convert(f32[32,256]{1,0:T(8,128)} %shard_map.181) | non-fusion elementwise | flops 8192 | bytes 49152 | tf_op jit(solution)/shard_map/convert_element_type | solution.py:569

commit v3 on v2

v3 whole, which is shorter than its diff:
```python
from typing import Any, NamedTuple

import jax
import jax.numpy as jnp
from jax import lax
from jax.experimental import pallas as pl
from jax.experimental.pallas import tpu as pltpu
from jax.sharding import PartitionSpec as P

EPS = 1e-06
LIMIT = 7.0
ALPHA = 1.702
MESH = pl.DeviceIdType.MESH
F32 = jnp.float32
BF16 = jnp.bfloat16
CHUNKS = 4
KEY_CHUNKS = 4
ROWS = 16
scope = jax.named_scope


class Args(NamedTuple):
    tokens: Any
    lengths: Any
    cache_keys: Any
    cache_values: Any
    attn_gain: Any
    q_first_w: Any
    q_second_w: Any
    k_first_w: Any
    k_second_w: Any
    value_w: Any
    mix_lambda: Any
    head_gain: Any
    out_w: Any
    ffn_gain: Any
    routes: Any
    route_logits: Any
    gate_w: Any
    up_w: Any
    down_w: Any


class Held(NamedTuple):
    tokens: Any
    lengths: Any
    cache_keys: Any
    cache_values: Any
    attn_gain: Any
    narrow_w: Any
    value_w: Any
    mix_lambda: Any
    head_gain: Any
    out_w: Any
    ffn_gain: Any
    routes: Any
    route_logits: Any
    gate_up_w: Any
    down_w: Any


class Loads(NamedTuple):
    tokens: Any
    attn_gain: Any
    narrow_w: Any
    lengths: Any
    mix_lambda: Any
    head_gain: Any
    value_w: Any
    ffn_gain: Any
    routes: Any
    route_logits: Any
    keys: Any
    values: Any
    out_w: Any
    gate_up_w: Any
    down_w: Any


class Work(NamedTuple):
    queries: Any
    scores: Any
    mixed: Any
    len_row: Any
    narrow: Any


class Bufs(NamedTuple):
    part: Any
    rs: Any
    a: Any
    x: Any
    p: Any
    hid: Any
    ret: Any
    fin: Any


class Pair(NamedTuple):
    send: Any
    recv: Any


class Sems(NamedTuple):
    idle: Any
    rs: Pair
    x: Pair
    p: Pair
    hy: Pair
    hd: Pair
    re: Pair


def dot(a, b):
    return jnp.dot(a, b, preferred_element_type=F32)


def dot_nt(a, b):
    return lax.dot_general(a, b, (((1,), (1,)), ((), ())), preferred_element_type=F32)


def iota(shape, dim):
    return lax.broadcasted_iota(jnp.int32, shape, dim)


def plan_loads(hbm, vm, sems):
    count = iter(range(N_LOADS))

    def copy(src, dst):
        return (pltpu.make_async_copy(src, dst, sems.at[next(count)]),)

    half = hbm.q_first_w.shape[0]
    rows = hbm.cache_keys.shape[1] // KEY_CHUNKS
    seqs = hbm.cache_keys.shape[0] // CHUNKS
    ff = hbm.gate_w.shape[2]
    narrow = (hbm.q_first_w, hbm.q_second_w, hbm.k_first_w, hbm.k_second_w)
    spans = [pl.ds(i * rows, rows) for i in range(KEY_CHUNKS)]
    blocks = [pl.ds(i * seqs, seqs) for i in range(CHUNKS)]
    return Loads(
        tokens=copy(hbm.tokens, vm.tokens),
        attn_gain=copy(hbm.attn_gain, vm.attn_gain),
        narrow_w=sum((copy(w, vm.narrow_w.at[pl.ds(i * half, half)]) for i, w in enumerate(narrow)), ()),
        lengths=copy(hbm.lengths, vm.lengths),
        mix_lambda=copy(hbm.mix_lambda, vm.mix_lambda),
        head_gain=copy(hbm.head_gain, vm.head_gain),
        value_w=copy(hbm.value_w, vm.value_w),
        ffn_gain=copy(hbm.ffn_gain, vm.ffn_gain),
        routes=copy(hbm.routes, vm.routes),
        route_logits=copy(hbm.route_logits, vm.route_logits),
        keys=sum((copy(hbm.cache_keys.at[:, s, :], vm.cache_keys.at[:, s, :]) for s in spans), ()),
        values=sum((copy(hbm.cache_values.at[b], vm.cache_values.at[b]) for b in blocks), ()),
        out_w=copy(hbm.out_w, vm.out_w),
        gate_up_w=copy(hbm.gate_w, vm.gate_up_w.at[:, :, pl.ds(0, ff)])
        + copy(hbm.up_w, vm.gate_up_w.at[:, :, pl.ds(ff, ff)]),
        down_w=copy(hbm.down_w, vm.down_w),
    )


N_LOADS = 17 + KEY_CHUNKS + CHUNKS


def wait(copies):
    for copy in copies:
        copy.wait()


def attend(loads, vm, work, part_ref):
    with scope("load"):
        wait(loads.tokens + loads.attn_gain)
    with scope("proj"):
        seqs, width = vm.tokens.shape
        length, dim = vm.cache_keys.shape[1:]
        half = dim // 2
        tok = vm.tokens[...].astype(F32)
        mean_sq = jnp.mean(tok * tok, axis=1, keepdims=True)
        normed = (tok * lax.rsqrt(mean_sq + EPS) * vm.attn_gain[...]).astype(BF16)
        wait(loads.narrow_w)
        wait(loads.lengths + loads.mix_lambda + loads.head_gain + loads.value_w)
        work.len_row[...] = jnp.zeros_like(work.len_row)
        work.narrow[...] = jnp.zeros_like(work.narrow)
        narrow = dot_nt(vm.narrow_w[...], normed).astype(BF16).astype(F32)
        for i in range(4):
            lane = i % 2 * half
            work.narrow[i * half : (i + 1) * half, lane : lane + seqs] = narrow[i * half : (i + 1) * half, :]
        for lane in (0, half):
            work.len_row[0:1, lane : lane + seqs] = vm.lengths[...]
        q_t = work.narrow[0:dim, :] * (half ** (-0.5))
        k_t = work.narrow[dim : 2 * dim, :]
        new_value = dot(normed, vm.value_w[...]).astype(BF16).astype(F32)
        owner = iota((dim, dim), 1) - jnp.where(iota((dim, dim), 0) < half, 0, half)
        for s in range(seqs):
            work.queries[s * dim : (s + 1) * dim, :] = jnp.where(owner == s, q_t, 0.0).astype(BF16)
        own = jnp.sum(q_t * k_t, axis=0, keepdims=True)
        lens = work.len_row[0:1, :]
    rows = length // KEY_CHUNKS
    top = own
    for i in range(KEY_CHUNKS):
        with scope("wk"):
            loads.keys[i].wait()
        with scope("qk"):
            got = 0.0
            for first in range(0, seqs, seqs // 1):
                mine = range(first, first + seqs // 1)
                keys = jnp.concatenate([vm.cache_keys[s, i * rows : (i + 1) * rows, :] for s in mine], axis=1)
                got = got + dot(keys, work.queries[first * dim : (first + seqs // 1) * dim, :])
            valid = iota((rows, dim), 0) + i * rows < lens
            got = jnp.where(valid, got, -jnp.inf)
            work.scores[i * rows : (i + 1) * rows, :] = got
            top = jnp.maximum(top, jnp.max(got, axis=0, keepdims=True))
    with scope("soft"):
        own_raised = jnp.exp(own - top)
        total = own_raised
        for i in range(KEY_CHUNKS):
            raised = jnp.exp(work.scores[i * rows : (i + 1) * rows, :] - top)
            work.scores[i * rows : (i + 1) * rows, :] = raised
            total = total + jnp.sum(raised, axis=0, keepdims=True)
        share = jnp.where(iota((1, dim), 1) < half, 1.0, -vm.mix_lambda[...]) / total
        for i in range(length // dim):
            block = (work.scores[i * dim : (i + 1) * dim, :] * share).T
            mixed = block[0:seqs, :] + block[half : half + seqs, :]
            work.mixed[:, i * dim : (i + 1) * dim] = mixed.astype(BF16)
        own_w = jnp.broadcast_to(own_raised * share, (dim, dim)).T
        own_col = (own_w[0:seqs, :] + own_w[half : half + seqs, :]).astype(BF16).astype(F32)
    group = 16
    place = iota((group, dim), 0)
    outs = [jnp.zeros((group, dim), F32) for _ in range(seqs // group)]
    per = seqs // CHUNKS
    for i in range(CHUNKS):
        with scope("wv"):
            loads.values[i].wait()
        with scope("pv"):
            for s in range(i * per, (i + 1) * per, 2):
                g = s // group
                both = jnp.concatenate([vm.cache_values[s], vm.cache_values[s + 1]], axis=1)
                got = dot(work.mixed[g * group : (g + 1) * group, :], both)
                outs[g] = outs[g] + jnp.where(place == s % group, got[:, 0:dim], 0.0)
                outs[g] = outs[g] + jnp.where(place == s % group + 1, got[:, dim : 2 * dim], 0.0)
    with scope("head"):
        head_out = jnp.concatenate(outs, axis=0) + own_col * new_value
        mean_sq = jnp.mean(head_out * head_out, axis=1, keepdims=True)
        attended = (head_out * lax.rsqrt(mean_sq + EPS) * vm.head_gain[...]).astype(BF16)
        wait(loads.out_w)
        blocks, _, cols = part_ref.shape
        for b in range(blocks):
            part_ref[b] = dot(attended, vm.out_w[:, b * cols : (b + 1) * cols]).astype(BF16)


def remote(src, dst, send, recv, ep, tp):
    return pltpu.make_async_remote_copy(
        src_ref=src, dst_ref=dst, send_sem=send, recv_sem=recv, device_id=(ep, tp), device_id_type=MESH
    )


def slot_tables(vm, slots):
    routes, logits = vm.routes[...], vm.route_logits[...]
    top, seqs = routes.shape
    logits = jnp.exp(logits - jnp.max(logits, axis=0, keepdims=True))
    weights = logits / jnp.sum(logits, axis=0, keepdims=True)
    slot = iota((slots, seqs), 0)
    half = slots // 2
    expert = slot % half // 8 * 4 + slot // half * 2 + slot % 8 // 4
    named = jnp.zeros((slots, seqs), F32)
    weight = jnp.zeros((slots, seqs), F32)
    for k in range(top):
        hit = routes[k : k + 1, :] == expert
        named = jnp.where(hit, 1.0, named)
        weight = jnp.where(hit, weights[k : k + 1, :], weight)
    before = (iota((seqs, seqs), 0) < iota((seqs, seqs), 1)).astype(F32).astype(BF16)
    rank = dot(named.astype(BF16), before)
    taken = (named > 0.5) & (rank == (slot % 4).astype(F32))
    return jnp.where(taken, 1.0, 0.0).astype(BF16), jnp.where(taken, weight, 0.0)


def far_first(sizes):
    every = [()]
    for n in sizes:
        every = [o + (d,) for o in every for d in range(n)]
    hops = lambda o: sum(min(d, n - d) for d, n in zip(o, sizes, strict=True))
    return sorted(every, key=hops, reverse=True)


def exchange(sizes, loads, vm, bufs, wide, sems, out_ref):
    n_ep, n_tp, owned = sizes
    n_y, n_x = n_tp // 2, 4
    n_z = n_ep // n_x
    e, t = lax.axis_index("ep"), lax.axis_index("tp")
    y, c = t // 2, t % 2
    z, x = e // n_x, e % n_x
    partner = t + 1 - 2 * c
    seqs, cols = bufs.part.shape[1:]
    slots = n_ep * ROWS
    half = slots // 2
    lanes = 128

    def ep_at(dz, dx):
        return (z + dz) % n_z * n_x + (x + dx) % n_x

    def tp_at(dy, dc):
        return (y + dy) % n_y * 2 + (c + dc) % 2

    def send(src, dst, sent, got, ep, tp):
        remote(src, dst, sent, got, ep, tp).start()

    def sent_all(buf, sem):
        remote(buf, buf, sem, sems.idle.at[0], e, partner).wait_send()

    def arrive(buf, sem):
        remote(buf, buf, sems.idle.at[0], sem, e, partner).wait_recv()

    with scope("rs"):
        for dy, dc in far_first((n_y, 2)):
            if dy or dc:
                to = tp_at(dy, dc)
                send(bufs.part.at[to], bufs.rs.at[t], sems.rs.send.at[0], sems.rs.recv.at[0], e, to)
        wait(loads.routes + loads.route_logits + loads.ffn_gain)
        dispatch, combine = slot_tables(vm, slots)
        wide[...] = jnp.zeros_like(wide)
        wide[:, 0:seqs] = combine
        combine = jnp.concatenate([wide[i : i + lanes, :].T[0:seqs, :] for i in range(0, slots, lanes)], axis=1)
        combine_hi = combine.astype(BF16)
        combine_lo = (combine - combine_hi.astype(F32)).astype(BF16)
        start = pl.multiple_of(t * cols, cols)
        kept = vm.tokens[:, pl.ds(start, cols)].astype(F32)
        gain = vm.ffn_gain[:, pl.ds(start, cols)]
        bufs.rs[t] = bufs.part[t]
    with scope("rsw"):
        arrive(bufs.rs.at[pl.ds(0, n_tp - 1)], sems.rs.recv.at[0])
        for i in range(n_tp):
            kept = kept + bufs.rs[i].astype(F32)

    with scope("d1"):
        rows = dot(dispatch, (kept * gain).astype(BF16)).astype(BF16)
        bufs.a[...] = rows.reshape(bufs.a.shape)
        for dz, dx, dy in far_first((n_z, n_x, n_y)):
            to = ep_at(dz, dx)
            if dz or dx or dy:
                which = 1 if dy else 0
                send(
                    bufs.a.at[:, to], bufs.x.at[:, y, e], sems.x.send.at[which], sems.x.recv.at[e], to, tp_at(dy, 0)
                )
        bufs.x[:, y, e] = bufs.a[:, e]
    with scope("xw"):
        for dz, dx in reversed(far_first((n_z, n_x))):
            frm = ep_at(dz, dx)
            arrive(bufs.x.at[:, pl.ds(0, n_y if dz or dx else n_y - 1), frm], sems.x.recv.at[frm])
            send(bufs.x.at[:, :, frm], bufs.p.at[:, :, frm], sems.p.send.at[0], sems.p.recv.at[0], e, partner)

    wait(loads.gate_up_w + loads.down_w)
    ff = vm.gate_up_w.shape[2] // 2
    odd = iota((half, 2 * ff), 0) % 8 // 4 == 1

    def gate_up(buf, core, h):
        squares = jnp.zeros((half, lanes), F32)
        tiles, begins = [], []
        for i in range(n_y):
            begin = pl.multiple_of((2 * i + core) * cols, cols)
            begins.append(begin)
            tile = buf[h, i].reshape(half, cols)
            tiles.append(tile)
            tile = tile.astype(F32) * (1.0 / vm.ffn_gain[:, pl.ds(begin, cols)])
            for j in range(0, cols, lanes):
                squares = squares + tile[:, j : j + lanes] * tile[:, j : j + lanes]
        tiles = jnp.concatenate(tiles, axis=1)
        got = [
            dot(tiles, jnp.concatenate([vm.gate_up_w[j, pl.ds(b, cols), :] for b in begins], axis=0))
            for j in (2 * h, 2 * h + 1)
        ]
        return jnp.where(odd, got[1], got[0]), squares

    with scope("gu"):
        firsts = [gate_up(bufs.x, c, h) for h in range(2)]
    with scope("pw"):
        arrive(bufs.p, sems.p.recv.at[0])
    for h in range(2):
        with scope("gv"):
            both, squares = gate_up(bufs.p, 1 - c, h)
            both, squares = both + firsts[h][0], squares + firsts[h][1]
            scale = lax.rsqrt(jnp.sum(squares, axis=1, keepdims=True) / (n_tp * cols) + EPS)
            both = both * scale
            gate = jnp.minimum(both[:, :ff], LIMIT)
            up = jnp.clip(both[:, ff:], -LIMIT, LIMIT)
            mine = bufs.hid.at[h, t]
            mine[...] = ((up + 1.0) * gate / (1.0 + jnp.exp(-ALPHA * gate))).astype(BF16)

            for (dy,) in far_first((n_y,)):
                if dy:
                    send(mine, mine, sems.hy.send.at[h], sems.hy.recv.at[h * n_y + y], e, tp_at(dy, 0))
            send(mine, mine, sems.hd.send.at[h], sems.hd.recv.at[h], e, partner)
    odd = iota((half, cols), 0) % 8 // 4 == 1
    with scope("hyw"):
        for h in range(2):
            for (dy,) in reversed(far_first((n_y,))):
                if dy:
                    frm = tp_at(dy, 0)
                    block = bufs.hid.at[h, frm]
                    arrive(block, sems.hy.recv.at[h * n_y + frm // 2])
                    send(block, block, sems.hd.send.at[h], sems.hd.recv.at[h], e, partner)
    for h in range(2):
        with scope("hdw"):
            arrive(bufs.hid.at[h, pl.ds(0, n_y)], sems.hd.recv.at[h])
        with scope("down"):
            hidden = jnp.concatenate([bufs.hid[h, i] for i in range(n_tp)], axis=1)
            result = jnp.where(odd, dot(hidden, vm.down_w[2 * h + 1]), dot(hidden, vm.down_w[2 * h]))
            bufs.ret[h] = result.astype(BF16).reshape(bufs.ret.shape[1:])

            for dz, dx in far_first((n_z, n_x)):
                if dz or dx:
                    to = ep_at(dz, dx)
                    send(bufs.ret.at[h, to], bufs.fin.at[h, e], sems.re.send.at[h], sems.re.recv.at[h], to, t)
            bufs.fin[h, e] = bufs.ret[h, e]
    with scope("rew"):
        for h in range(2):
            arrive(bufs.fin.at[h, pl.ds(0, n_ep - 1)], sems.re.recv.at[h])
    with scope("fin"):
        back = bufs.fin[...].reshape(slots, cols)
        out_ref[...] = (kept + dot(combine_hi, back) + dot(combine_lo, back)).astype(out_ref.dtype)
        sent_all(bufs.part.at[pl.ds(0, n_tp - 1)], sems.rs.send.at[0])
        sent_all(bufs.x.at[:, 0, pl.ds(0, n_ep - 1)], sems.x.send.at[0])
        sent_all(bufs.x.at[:, pl.ds(0, n_y - 1)], sems.x.send.at[1])
        sent_all(bufs.x, sems.p.send.at[0])
        for h in range(2):
            sent_all(bufs.hid.at[h, pl.ds(0, n_y - 1)], sems.hy.send.at[h])
            sent_all(bufs.hid.at[h, pl.ds(0, n_y)], sems.hd.send.at[h])
            sent_all(bufs.ret.at[h, pl.ds(0, n_ep - 1)], sems.re.send.at[h])


def buffers(n_ep, n_tp, seqs, cols, ff):
    n_y, rows = n_tp // 2, ROWS // 2

    def array(*shape):
        return pltpu.VMEM(shape, BF16)

    return Bufs(
        part=array(n_tp, seqs, cols),
        rs=array(n_tp, seqs, cols),
        a=array(2, n_ep, rows, cols),
        x=array(2, n_y, n_ep, rows, cols),
        p=array(2, n_y, n_ep, rows, cols),
        hid=array(2, n_tp, n_ep * rows, ff),
        ret=array(2, n_ep, rows, cols),
        fin=array(2, n_ep, rows, cols),
    )


def semaphores(n_ep, n_tp):
    def pair(sends, recvs):
        return Pair(pltpu.SemaphoreType.DMA((sends,)), pltpu.SemaphoreType.DMA((recvs,)))

    return Sems(
        idle=pltpu.SemaphoreType.DMA((1,)),
        rs=pair(1, 1),
        x=pair(2, n_ep),
        p=pair(1, 1),
        hy=pair(2, n_tp),
        hd=pair(2, 2),
        re=pair(2, 2),
    )


def run(n_ep, n_tp, hbm):
    seqs, width = hbm.tokens.shape
    length, dim = hbm.cache_keys.shape[1:]
    owned, _, ff = hbm.gate_w.shape
    cols = width // n_tp
    hbm = hbm._replace(
        lengths=hbm.lengths.reshape(1, -1),
        attn_gain=hbm.attn_gain.reshape(1, -1),
        head_gain=hbm.head_gain.reshape(1, -1),
        ffn_gain=hbm.ffn_gain.reshape(1, -1),
        mix_lambda=hbm.mix_lambda.reshape(1, -1),
        q_first_w=hbm.q_first_w.T,
        q_second_w=hbm.q_second_w.T,
        k_first_w=hbm.k_first_w.T,
        k_second_w=hbm.k_second_w.T,
        routes=hbm.routes.T,
        route_logits=hbm.route_logits.T,
    )

    def like(x):
        return pltpu.VMEM(x.shape, x.dtype)

    vm = Held(
        tokens=like(hbm.tokens),
        lengths=like(hbm.lengths),
        cache_keys=like(hbm.cache_keys),
        cache_values=like(hbm.cache_values),
        attn_gain=like(hbm.attn_gain),
        narrow_w=pltpu.VMEM((2 * dim, width), BF16),
        value_w=like(hbm.value_w),
        mix_lambda=like(hbm.mix_lambda),
        head_gain=like(hbm.head_gain),
        out_w=like(hbm.out_w),
        ffn_gain=like(hbm.ffn_gain),
        routes=like(hbm.routes),
        route_logits=like(hbm.route_logits),
        gate_up_w=pltpu.VMEM((owned, width, 2 * ff), BF16),
        down_w=like(hbm.down_w),
    )
    work = Work(
        queries=pltpu.VMEM((seqs * dim, dim), BF16),
        scores=pltpu.VMEM((length, dim), F32),
        mixed=pltpu.VMEM((seqs, length), BF16),
        len_row=pltpu.VMEM((8, dim), jnp.int32),
        narrow=pltpu.VMEM((2 * dim, dim), F32),
    )

    def kernel(hbm, out_ref, vm, work, bufs, wide, sems, load_sems):
        loads = plan_loads(hbm, vm, load_sems)
        for group in loads:
            for copy in group:
                copy.start()
        e, t = lax.axis_index("ep"), lax.axis_index("tp")
        barrier = pltpu.get_barrier_semaphore()
        for k in range(1, n_tp):
            pl.semaphore_signal(barrier, inc=1, device_id=(e, (t + k) % n_tp), device_id_type=MESH)
        for k in range(1, n_ep):
            pl.semaphore_signal(barrier, inc=1, device_id=((e + k) % n_ep, t), device_id_type=MESH)
        attend(loads, vm, work, bufs.part)
        with scope("bar"):
            pl.semaphore_wait(barrier, n_tp + n_ep - 2)
        exchange((n_ep, n_tp, owned), loads, vm, bufs, wide, sems, out_ref)

    return pl.pallas_call(
        kernel,
        out_shape=pltpu.VMEM((seqs, cols), OUT),
        in_specs=[Args(*[pl.BlockSpec(memory_space=pl.ANY)] * len(hbm))],
        out_specs=pl.BlockSpec(memory_space=pltpu.VMEM),
        scratch_shapes=[
            vm,
            work,
            buffers(n_ep, n_tp, seqs, cols, ff),
            pltpu.VMEM((n_ep * ROWS, 128), F32),
            semaphores(n_ep, n_tp),
            pltpu.SemaphoreType.DMA((N_LOADS,)),
        ],
        compiler_params=pltpu.CompilerParams(
            vmem_limit_bytes=56 * 1024 * 1024, collective_id=0, has_side_effects=True
        ),
    )(hbm)


OUT = F32


def solution(mesh):
    n_ep, n_tp = mesh.shape["ep"], mesh.shape["tp"]

    def per_device(*args):
        return run(n_ep, n_tp, Args(*args)).astype(BF16)

    rows, heads, both = P("ep", None), P(None, "tp"), P("ep", None, "tp")
    return jax.shard_map(
        per_device,
        mesh=mesh,
        in_specs=(
            rows, P("ep"), both, both, P(), heads, heads, heads, heads, heads,
            P("tp"), P(), P("tp", None), P(), rows, rows, both, both, both,
        ),
        out_specs=P("ep", "tp"),
        check_vma=False,
    )
```

time: 47.5 us -> 40.5 us (0.85)
  Pallas kernels: 45.1 us -> 38.8 us
  other arithmetic: 1.37 us -> 0.61 us
    pallas_call x1, Pallas kernels: 45.1 us -> 38.8 us  [run(): pl.pallas_call(kernel, out_shape=pltpu.VMEM((seqs, cols), OUT), in_specs=...]
    convert_element_type x1, other arithmetic: 1.37 us -> 0.61 us  [per_device(): return run(n_ep, n_tp, Args(*args)).astype(BF16)]
where the time goes in v3:
time: 40.5 us; the launch traced here: 40 us
  Pallas kernels  38.8 us (96%)
  between operations  0.66 us (2%)
  other arithmetic  0.61 us (2%)
    pallas_call x1, Pallas kernels, run(): pl.pallas_call(kernel, out_shape=pltpu.VMEM((seqs, cols), OUT), in_specs=...  38.8 us

profile of v3, /device:TPU:0, one launch (start us, length us, event | category | flops | bytes accessed | tf_op | source)
XLA Modules:
  0.0 40.0 jit_solution(7002751824881854342)
XLA Ops:
  0.7 38.8 %shard_map.181 = f32[32,256]{1,0:T(8,128)S(1)} custom-call(bf16[32,2048]{1,0:T(8,128)(2,1)} %hbm_tokens.1, s32[1,32]{1,0:T(1,128)} %bitcast.20, bf16[32,1024,128]{2,1,0:T(8,128)(2,1)} %hbm_cache_keys.1, bf16[32,1024,128]{2,1,0:T(8,128)(2,1)} %hbm_cache_values.1, f32[1,2048]{1,0:T(1,128)} %bitcast.16, bf16[64,2048]{1,0:T(8,128)(2,1)} %bitcast.12, ...), custom_call_target="tpu_custom_call" | custom-call | tf_op jit(solution)/shard_map/pallas_call | solution.py:523
  39.4 0.6 %convert_element_type.3 = bf16[32,256]{1,0:T(8,128)(2,1)} convert(f32[32,256]{1,0:T(8,128)S(1)} %shard_map.181) | non-fusion elementwise | flops 8192 | bytes 49152 | tf_op jit(solution)/shard_map/convert_element_type | solution.py:549

commit v4 on v3

--- a/solution.py
+++ b/solution.py
@@ -13,9 +13,10 @@
 MESH = pl.DeviceIdType.MESH
 F32 = jnp.float32
 BF16 = jnp.bfloat16
-CHUNKS = 4
+CHUNKS = 2
 KEY_CHUNKS = 4
 ROWS = 16
+EARLY = (0, 1, 2, 3, 4, 8)
 scope = jax.named_scope
 
 
@@ -91,7 +92,8 @@
     a: Any
     x: Any
     p: Any
-    hid: Any
+    hid_a: Any
+    hid_b: Any
     ret: Any
     fin: Any
 
@@ -123,11 +125,27 @@
     return lax.broadcasted_iota(jnp.int32, shape, dim)
 
 
+class Pieces(NamedTuple):
+    copies: Any
+    whole: Any
+
+    def start(self):
+        for copy in self.copies:
+            copy.start()
+
+    def wait(self):
+        self.whole.wait()
+
+
 def plan_loads(hbm, vm, sems):
     count = iter(range(N_LOADS))
 
     def copy(src, dst):
         return (pltpu.make_async_copy(src, dst, sems.at[next(count)]),)
+
+    def pieces(whole, parts):
+        sem = sems.at[next(count)]
+        return Pieces([pltpu.make_async_copy(s, d, sem) for s, d in parts], pltpu.make_async_copy(whole, whole, sem))
 
     half = hbm.q_first_w.shape[0]
     rows = hbm.cache_keys.shape[1] // KEY_CHUNKS
@@ -139,7 +157,9 @@
     return Loads(
         tokens=copy(hbm.tokens, vm.tokens),
         attn_gain=copy(hbm.attn_gain, vm.attn_gain),
-        narrow_w=sum((copy(w, vm.narrow_w.at[pl.ds(i * half, half)]) for i, w in enumerate(narrow)), ()),
+        narrow_w=(
+            pieces(vm.narrow_w, [(w, vm.narrow_w.at[pl.ds(i * half, half)]) for i, w in enumerate(narrow)]),
+        ),
         lengths=copy(hbm.lengths, vm.lengths),
         mix_lambda=copy(hbm.mix_lambda, vm.mix_lambda),
         head_gain=copy(hbm.head_gain, vm.head_gain),
@@ -150,13 +170,17 @@
         keys=sum((copy(hbm.cache_keys.at[:, s, :], vm.cache_keys.at[:, s, :]) for s in spans), ()),
         values=sum((copy(hbm.cache_values.at[b], vm.cache_values.at[b]) for b in blocks), ()),
         out_w=copy(hbm.out_w, vm.out_w),
-        gate_up_w=copy(hbm.gate_w, vm.gate_up_w.at[:, :, pl.ds(0, ff)])
-        + copy(hbm.up_w, vm.gate_up_w.at[:, :, pl.ds(ff, ff)]),
+        gate_up_w=(
+            pieces(
+                vm.gate_up_w,
+                [(hbm.gate_w, vm.gate_up_w.at[:, :, pl.ds(0, ff)]), (hbm.up_w, vm.gate_up_w.at[:, :, pl.ds(ff, ff)])],
+            ),
+        ),
         down_w=copy(hbm.down_w, vm.down_w),
     )
 
 
-N_LOADS = 17 + KEY_CHUNKS + CHUNKS
+N_LOADS = 13 + KEY_CHUNKS + CHUNKS
 
 
 def wait(copies):
@@ -175,7 +199,7 @@
         mean_sq = jnp.mean(tok * tok, axis=1, keepdims=True)
         normed = (tok * lax.rsqrt(mean_sq + EPS) * vm.attn_gain[...]).astype(BF16)
         wait(loads.narrow_w)
-        wait(loads.lengths + loads.mix_lambda + loads.head_gain + loads.value_w)
+        wait(loads.lengths)
         work.len_row[...] = jnp.zeros_like(work.len_row)
         work.narrow[...] = jnp.zeros_like(work.narrow)
         narrow = dot_nt(vm.narrow_w[...], normed).astype(BF16).astype(F32)
@@ -186,7 +210,6 @@
             work.len_row[0:1, lane : lane + seqs] = vm.lengths[...]
         q_t = work.narrow[0:dim, :] * (half ** (-0.5))
         k_t = work.narrow[dim : 2 * dim, :]
-        new_value = dot(normed, vm.value_w[...]).astype(BF16).astype(F32)
         owner = iota((dim, dim), 1) - jnp.where(iota((dim, dim), 0) < half, 0, half)
         for s in range(seqs):
             work.queries[s * dim : (s + 1) * dim, :] = jnp.where(owner == s, q_t, 0.0).astype(BF16)
@@ -208,6 +231,8 @@
             work.scores[i * rows : (i + 1) * rows, :] = got
             top = jnp.maximum(top, jnp.max(got, axis=0, keepdims=True))
     with scope("soft"):
+        wait(loads.mix_lambda + loads.value_w)
+        new_value = dot(normed, vm.value_w[...]).astype(BF16).astype(F32)
         own_raised = jnp.exp(own - top)
         total = own_raised
         for i in range(KEY_CHUNKS):
@@ -236,6 +261,7 @@
                 outs[g] = outs[g] + jnp.where(place == s % group, got[:, 0:dim], 0.0)
                 outs[g] = outs[g] + jnp.where(place == s % group + 1, got[:, dim : 2 * dim], 0.0)
     with scope("head"):
+        wait(loads.head_gain)
         head_out = jnp.concatenate(outs, axis=0) + own_col * new_value
         mean_sq = jnp.mean(head_out * head_out, axis=1, keepdims=True)
         attended = (head_out * lax.rsqrt(mean_sq + EPS) * vm.head_gain[...]).astype(BF16)
@@ -257,12 +283,10 @@
     logits = jnp.exp(logits - jnp.max(logits, axis=0, keepdims=True))
     weights = logits / jnp.sum(logits, axis=0, keepdims=True)
     slot = iota((slots, seqs), 0)
-    half = slots // 2
-    expert = slot % half // 8 * 4 + slot // half * 2 + slot % 8 // 4
     named = jnp.zeros((slots, seqs), F32)
     weight = jnp.zeros((slots, seqs), F32)
     for k in range(top):
-        hit = routes[k : k + 1, :] == expert
+        hit = routes[k : k + 1, :] == slot // 4
         named = jnp.where(hit, 1.0, named)
         weight = jnp.where(hit, weights[k : k + 1, :], weight)
     before = (iota((seqs, seqs), 0) < iota((seqs, seqs), 1)).astype(F32).astype(BF16)
@@ -289,7 +313,6 @@
     partner = t + 1 - 2 * c
     seqs, cols = bufs.part.shape[1:]
     slots = n_ep * ROWS
-    half = slots // 2
     lanes = 128
 
     def ep_at(dz, dx):
@@ -335,27 +358,27 @@
             to = ep_at(dz, dx)
             if dz or dx or dy:
                 which = 1 if dy else 0
-                send(
-                    bufs.a.at[:, to], bufs.x.at[:, y, e], sems.x.send.at[which], sems.x.recv.at[e], to, tp_at(dy, 0)
-                )
-        bufs.x[:, y, e] = bufs.a[:, e]
-    with scope("xw"):
-        for dz, dx in reversed(far_first((n_z, n_x))):
-            frm = ep_at(dz, dx)
-            arrive(bufs.x.at[:, pl.ds(0, n_y if dz or dx else n_y - 1), frm], sems.x.recv.at[frm])
-            send(bufs.x.at[:, :, frm], bufs.p.at[:, :, frm], sems.p.send.at[0], sems.p.recv.at[0], e, partner)
-
-    wait(loads.gate_up_w + loads.down_w)
+                send(bufs.a.at[to], bufs.x.at[y, e], sems.x.send.at[which], sems.x.recv.at[e], to, tp_at(dy, 0))
+        bufs.x[y, e] = bufs.a[e]
+
+    halves = (EARLY, [g for g in range(n_ep) if g not in EARLY])
+    hids = (bufs.hid_a, bufs.hid_b)
     ff = vm.gate_up_w.shape[2] // 2
-    odd = iota((half, 2 * ff), 0) % 8 // 4 == 1
-
-    def gate_up(buf, core, h):
-        squares = jnp.zeros((half, lanes), F32)
+
+    def of_expert(results):
+        expert = iota(results[0].shape, 0) % ROWS // 4
+        total = results[0]
+        for j in range(1, owned):
+            total = jnp.where(expert == j, results[j], total)
+        return total
+
+    def gate_up(buf, core, groups):
+        squares = jnp.zeros((len(groups) * ROWS, lanes), F32)
         tiles, begins = [], []
         for i in range(n_y):
             begin = pl.multiple_of((2 * i + core) * cols, cols)
             begins.append(begin)
-            tile = buf[h, i].reshape(half, cols)
+            tile = jnp.concatenate([buf[i, g] for g in groups], axis=0)
             tiles.append(tile)
             tile = tile.astype(F32) * (1.0 / vm.ffn_gain[:, pl.ds(begin, cols)])
             for j in range(0, cols, lanes):
@@ -363,69 +386,86 @@
         tiles = jnp.concatenate(tiles, axis=1)
         got = [
             dot(tiles, jnp.concatenate([vm.gate_up_w[j, pl.ds(b, cols), :] for b in begins], axis=0))
-            for j in (2 * h, 2 * h + 1)
+            for j in range(owned)
         ]
-        return jnp.where(odd, got[1], got[0]), squares
-
-    with scope("gu"):
-        firsts = [gate_up(bufs.x, c, h) for h in range(2)]
-    with scope("pw"):
-        arrive(bufs.p, sems.p.recv.at[0])
-    for h in range(2):
+        return of_expert(got), squares
+
+    for h, groups in enumerate(halves):
+        with scope("xw"):
+            for g in groups:
+
+                @pl.when(e != g)
+                def _():
+                    arrive(bufs.x.at[pl.ds(0, n_y), g], sems.x.recv.at[g])
+
+                @pl.when(e == g)
+                def _():
+                    arrive(bufs.x.at[pl.ds(0, n_y - 1), g], sems.x.recv.at[g])
+
+                send(bufs.x.at[:, g], bufs.p.at[:, g], sems.p.send.at[0], sems.p.recv.at[h], e, partner)
+        if h == 0:
+            wait(loads.gate_up_w + loads.down_w)
+        with scope("gu"):
+            first, first_squares = gate_up(bufs.x, c, groups)
+        with scope("pw"):
+            arrive(bufs.p.at[:, pl.ds(0, len(groups))], sems.p.recv.at[h])
         with scope("gv"):
-            both, squares = gate_up(bufs.p, 1 - c, h)
-            both, squares = both + firsts[h][0], squares + firsts[h][1]
+            both, squares = gate_up(bufs.p, 1 - c, groups)
+            both, squares = both + first, squares + first_squares
             scale = lax.rsqrt(jnp.sum(squares, axis=1, keepdims=True) / (n_tp * cols) + EPS)
             both = both * scale
             gate = jnp.minimum(both[:, :ff], LIMIT)
             up = jnp.clip(both[:, ff:], -LIMIT, LIMIT)
-            mine = bufs.hid.at[h, t]
+            mine = hids[h].at[t]
             mine[...] = ((up + 1.0) * gate / (1.0 + jnp.exp(-ALPHA * gate))).astype(BF16)
 
             for (dy,) in far_first((n_y,)):
                 if dy:
-                    send(mine, mine, sems.hy.send.at[h], sems.hy.recv.at[h * n_y + y], e, tp_at(dy, 0))
+                    send(mine, mine, sems.hy.send.at[h], sems.hy.recv.at[h * (n_y - 1) + dy - 1], e, tp_at(dy, 0))
             send(mine, mine, sems.hd.send.at[h], sems.hd.recv.at[h], e, partner)
-    odd = iota((half, cols), 0) % 8 // 4 == 1
-    with scope("hyw"):
-        for h in range(2):
+    for h, groups in enumerate(halves):
+        with scope("hyw"):
             for (dy,) in reversed(far_first((n_y,))):
                 if dy:
                     frm = tp_at(dy, 0)
-                    block = bufs.hid.at[h, frm]
-                    arrive(block, sems.hy.recv.at[h * n_y + frm // 2])
+                    block = hids[h].at[frm]
+                    arrive(block, sems.hy.recv.at[h * (n_y - 1) + n_y - dy - 1])
                     send(block, block, sems.hd.send.at[h], sems.hd.recv.at[h], e, partner)
-    for h in range(2):
         with scope("hdw"):
-            arrive(bufs.hid.at[h, pl.ds(0, n_y)], sems.hd.recv.at[h])
+            arrive(hids[h].at[pl.ds(0, n_y)], sems.hd.recv.at[h])
         with scope("down"):
-            hidden = jnp.concatenate([bufs.hid[h, i] for i in range(n_tp)], axis=1)
-            result = jnp.where(odd, dot(hidden, vm.down_w[2 * h + 1]), dot(hidden, vm.down_w[2 * h]))
-            bufs.ret[h] = result.astype(BF16).reshape(bufs.ret.shape[1:])
-
-            for dz, dx in far_first((n_z, n_x)):
-                if dz or dx:
-                    to = ep_at(dz, dx)
-                    send(bufs.ret.at[h, to], bufs.fin.at[h, e], sems.re.send.at[h], sems.re.recv.at[h], to, t)
-            bufs.fin[h, e] = bufs.ret[h, e]
+            hidden = jnp.concatenate([hids[h][i] for i in range(n_tp)], axis=1)
+            result = of_expert([dot(hidden, vm.down_w[j]) for j in range(owned)]).astype(BF16)
+
+            for i, g in enumerate(groups):
+                bufs.ret[g] = result[i * ROWS : (i + 1) * ROWS, :]
+            for g in reversed(groups):
+
+                @pl.when(e != g)
+                def _():
+                    send(bufs.ret.at[g], bufs.fin.at[e], sems.re.send.at[0], sems.re.recv.at[0], g, t)
+
+                @pl.when(e == g)
+                def _():
+                    bufs.fin[g] = bufs.ret[g]
+
     with scope("rew"):
-        for h in range(2):
-            arrive(bufs.fin.at[h, pl.ds(0, n_ep - 1)], sems.re.recv.at[h])
+        arrive(bufs.fin.at[pl.ds(0, n_ep - 1)], sems.re.recv.at[0])
     with scope("fin"):
         back = bufs.fin[...].reshape(slots, cols)
         out_ref[...] = (kept + dot(combine_hi, back) + dot(combine_lo, back)).astype(out_ref.dtype)
         sent_all(bufs.part.at[pl.ds(0, n_tp - 1)], sems.rs.send.at[0])
-        sent_all(bufs.x.at[:, 0, pl.ds(0, n_ep - 1)], sems.x.send.at[0])
-        sent_all(bufs.x.at[:, pl.ds(0, n_y - 1)], sems.x.send.at[1])
+        sent_all(bufs.x.at[0, pl.ds(0, n_ep - 1)], sems.x.send.at[0])
+        sent_all(bufs.x.at[pl.ds(0, n_y - 1)], sems.x.send.at[1])
         sent_all(bufs.x, sems.p.send.at[0])
         for h in range(2):
-            sent_all(bufs.hid.at[h, pl.ds(0, n_y - 1)], sems.hy.send.at[h])
-            sent_all(bufs.hid.at[h, pl.ds(0, n_y)], sems.hd.send.at[h])
-            sent_all(bufs.ret.at[h, pl.ds(0, n_ep - 1)], sems.re.send.at[h])
+            sent_all(hids[h].at[pl.ds(0, n_y - 1)], sems.hy.send.at[h])
+            sent_all(hids[h].at[pl.ds(0, n_y)], sems.hd.send.at[h])
+        sent_all(bufs.ret.at[pl.ds(0, n_ep - 1)], sems.re.send.at[0])
 
 
 def buffers(n_ep, n_tp, seqs, cols, ff):
-    n_y, rows = n_tp // 2, ROWS // 2
+    n_y = n_tp // 2
 
     def array(*shape):
         return pltpu.VMEM(shape, BF16)
@@ -433,12 +473,13 @@
     return Bufs(
         part=array(n_tp, seqs, cols),
         rs=array(n_tp, seqs, cols),
-        a=array(2, n_ep, rows, cols),
-        x=array(2, n_y, n_ep, rows, cols),
-        p=array(2, n_y, n_ep, rows, cols),
-        hid=array(2, n_tp, n_ep * rows, ff),
-        ret=array(2, n_ep, rows, cols),
-        fin=array(2, n_ep, rows, cols),
+        a=array(n_ep, ROWS, cols),
+        x=array(n_y, n_ep, ROWS, cols),
+        p=array(n_y, n_ep, ROWS, cols),
+        hid_a=array(n_tp, len(EARLY) * ROWS, ff),
+        hid_b=array(n_tp, (n_ep - len(EARLY)) * ROWS, ff),
+        ret=array(n_ep, ROWS, cols),
+        fin=array(n_ep, ROWS, cols),
     )
 
 
@@ -450,10 +491,10 @@
         idle=pltpu.SemaphoreType.DMA((1,)),
         rs=pair(1, 1),
         x=pair(2, n_ep),
-        p=pair(1, 1),
-        hy=pair(2, n_tp),
+        p=pair(1, 2),
+        hy=pair(2, n_tp - 2),
         hd=pair(2, 2),
-        re=pair(2, 2),
+        re=pair(1, 1),
     )
 
 

time: 40.5 us -> 37.6 us (0.928)
  the two profiles are of different devices: /device:TPU:0 before, /device:TPU:1 now
where the time goes in v4:
time: 37.6 us; the launch traced here: 37.5 us
  Pallas kernels  36.2 us (96%)
  between operations  0.66 us (2%)
  other arithmetic  0.61 us (2%)
    pallas_call x1, Pallas kernels, run(): pl.pallas_call(kernel, out_shape=pltpu.VMEM((seqs, cols), OUT), in_specs=...  36.2 us

profile of v4, /device:TPU:1, one launch (start us, length us, event | category | flops | bytes accessed | tf_op | source)
XLA Modules:
  0.0 37.5 jit_solution(14984733589407967311)
XLA Ops:
  0.7 36.2 %shard_map.181 = f32[32,256]{1,0:T(8,128)S(1)} custom-call(bf16[32,2048]{1,0:T(8,128)(2,1)} %hbm_tokens.1, s32[1,32]{1,0:T(1,128)} %bitcast.20, bf16[32,1024,128]{2,1,0:T(8,128)(2,1)} %hbm_cache_keys.1, bf16[32,1024,128]{2,1,0:T(8,128)(2,1)} %hbm_cache_values.1, f32[1,2048]{1,0:T(1,128)} %bitcast.16, bf16[64,2048]{1,0:T(8,128)(2,1)} %bitcast.12, ...), custom_call_target="tpu_custom_call" | custom-call | tf_op jit(solution)/shard_map/pallas_call | solution.py:564
  36.9 0.6 %convert_element_type.3 = bf16[32,256]{1,0:T(8,128)(2,1)} convert(f32[32,256]{1,0:T(8,128)S(1)} %shard_map.181) | non-fusion elementwise | flops 8192 | bytes 49152 | tf_op jit(solution)/shard_map/convert_element_type | solution.py:590

commit v5 on v4

--- a/solution.py
+++ b/solution.py
@@ -319,7 +319,7 @@
         return (z + dz) % n_z * n_x + (x + dx) % n_x
 
     def tp_at(dy, dc):
-        return (y + dy) % n_y * 2 + (c + dc) % 2
+        return (y + dy) % n_y * 2 + (c + dc + 2) % 2
 
     def send(src, dst, sent, got, ep, tp):
         remote(src, dst, sent, got, ep, tp).start()
@@ -421,18 +421,25 @@
 
             for (dy,) in far_first((n_y,)):
                 if dy:
-                    send(mine, mine, sems.hy.send.at[h], sems.hy.recv.at[h * (n_y - 1) + dy - 1], e, tp_at(dy, 0))
+                    place = (h * (n_y - 1) + dy - 1) * 2 + c
+                    send(mine, mine, sems.hy.send.at[h], sems.hy.recv.at[place], e, tp_at(dy, 1 - c))
             send(mine, mine, sems.hd.send.at[h], sems.hd.recv.at[h], e, partner)
     for h, groups in enumerate(halves):
         with scope("hyw"):
-            for (dy,) in reversed(far_first((n_y,))):
-                if dy:
-                    frm = tp_at(dy, 0)
-                    block = hids[h].at[frm]
-                    arrive(block, sems.hy.recv.at[h * (n_y - 1) + n_y - dy - 1])
-                    send(block, block, sems.hd.send.at[h], sems.hd.recv.at[h], e, partner)
-        with scope("hdw"):
-            arrive(hids[h].at[pl.ds(0, n_y)], sems.hd.recv.at[h])
+
+            @pl.when(c == 1)
+            def _():
+                for (dy,) in reversed(far_first((n_y,))):
+                    for core in (1, 0) if dy else ():
+                        block = hids[h].at[tp_at(dy, core - c)]
+                        arrive(block, sems.hy.recv.at[(h * (n_y - 1) + n_y - dy - 1) * 2 + core])
+                        send(block, block, sems.hd.send.at[h], sems.hd.recv.at[h], e, partner)
+                arrive(hids[h].at[0], sems.hd.recv.at[h])
+
+            @pl.when(c == 0)
+            def _():
+                arrive(hids[h].at[pl.ds(0, n_tp - 1)], sems.hd.recv.at[h])
+
         with scope("down"):
             hidden = jnp.concatenate([hids[h][i] for i in range(n_tp)], axis=1)
             result = of_expert([dot(hidden, vm.down_w[j]) for j in range(owned)]).astype(BF16)
@@ -460,7 +467,15 @@
         sent_all(bufs.x, sems.p.send.at[0])
         for h in range(2):
             sent_all(hids[h].at[pl.ds(0, n_y - 1)], sems.hy.send.at[h])
-            sent_all(hids[h].at[pl.ds(0, n_y)], sems.hd.send.at[h])
+
+            @pl.when(c == 1)
+            def _():
+                sent_all(hids[h].at[pl.ds(0, n_tp - 1)], sems.hd.send.at[h])
+
+            @pl.when(c == 0)
+            def _():
+                sent_all(hids[h].at[0], sems.hd.send.at[h])
+
         sent_all(bufs.ret.at[pl.ds(0, n_ep - 1)], sems.re.send.at[0])
 
 
@@ -492,7 +507,7 @@
         rs=pair(1, 1),
         x=pair(2, n_ep),
         p=pair(1, 2),
-        hy=pair(2, n_tp - 2),
+        hy=pair(2, 2 * (n_tp - 2)),
         hd=pair(2, 2),
         re=pair(1, 1),
     )

time: 37.6 us -> 37.2 us (0.989)
  the two profiles are of different devices: /device:TPU:1 before, /device:TPU:0 now
where the time goes in v5:
time: 37.2 us; the launch traced here: 36.6 us
  Pallas kernels  35.3 us (95%)
  between operations  0.66 us (2%)
  other arithmetic  0.61 us (2%)
    pallas_call x1, Pallas kernels, run(): pl.pallas_call(kernel, out_shape=pltpu.VMEM((seqs, cols), OUT), in_specs=...  35.3 us

profile of v5, /device:TPU:0, one launch (start us, length us, event | category | flops | bytes accessed | tf_op | source)
XLA Modules:
  0.0 36.6 jit_solution(14954293123203499723)
XLA Ops:
  0.7 35.3 %shard_map.181 = f32[32,256]{1,0:T(8,128)S(1)} custom-call(bf16[32,2048]{1,0:T(8,128)(2,1)} %hbm_tokens.1, s32[1,32]{1,0:T(1,128)} %bitcast.20, bf16[32,1024,128]{2,1,0:T(8,128)(2,1)} %hbm_cache_keys.1, bf16[32,1024,128]{2,1,0:T(8,128)(2,1)} %hbm_cache_values.1, f32[1,2048]{1,0:T(1,128)} %bitcast.16, bf16[64,2048]{1,0:T(8,128)(2,1)} %bitcast.12, ...), custom_call_target="tpu_custom_call" | custom-call | tf_op jit(solution)/shard_map/pallas_call | solution.py:579
  36.0 0.6 %convert_element_type.3 = bf16[32,256]{1,0:T(8,128)(2,1)} convert(f32[32,256]{1,0:T(8,128)S(1)} %shard_map.181) | non-fusion elementwise | flops 8192 | bytes 49152 | tf_op jit(solution)/shard_map/convert_element_type | solution.py:605

commit v6 on v5

--- a/solution.py
+++ b/solution.py
@@ -1,3 +1,4 @@
+import itertools
 from typing import Any, NamedTuple
 
 import jax
@@ -13,10 +14,11 @@
 MESH = pl.DeviceIdType.MESH
 F32 = jnp.float32
 BF16 = jnp.bfloat16
-CHUNKS = 2
+VALUE_CUTS = (0, 16, 28, 32)
 KEY_CHUNKS = 4
 ROWS = 16
-EARLY = (0, 1, 2, 3, 4, 8)
+SETS = ((0, 1, 2), (3, 4, 8)), ((5, 6, 7, 9), (10, 11, 12), (13, 14, 15))
+EARLY = sum(SETS[0], ())
 scope = jax.named_scope
 
 
@@ -149,11 +151,10 @@
 
     half = hbm.q_first_w.shape[0]
     rows = hbm.cache_keys.shape[1] // KEY_CHUNKS
-    seqs = hbm.cache_keys.shape[0] // CHUNKS
     ff = hbm.gate_w.shape[2]
     narrow = (hbm.q_first_w, hbm.q_second_w, hbm.k_first_w, hbm.k_second_w)
     spans = [pl.ds(i * rows, rows) for i in range(KEY_CHUNKS)]
-    blocks = [pl.ds(i * seqs, seqs) for i in range(CHUNKS)]
+    blocks = [pl.ds(a, b - a) for a, b in itertools.pairwise(VALUE_CUTS)]
     return Loads(
         tokens=copy(hbm.tokens, vm.tokens),
         attn_gain=copy(hbm.attn_gain, vm.attn_gain),
@@ -180,7 +181,7 @@
     )
 
 
-N_LOADS = 13 + KEY_CHUNKS + CHUNKS
+N_LOADS = 12 + KEY_CHUNKS + len(VALUE_CUTS)
 
 
 def wait(copies):
@@ -249,12 +250,11 @@
     group = 16
     place = iota((group, dim), 0)
     outs = [jnp.zeros((group, dim), F32) for _ in range(seqs // group)]
-    per = seqs // CHUNKS
-    for i in range(CHUNKS):
+    for i, (start, stop) in enumerate(itertools.pairwise(VALUE_CUTS)):
         with scope("wv"):
             loads.values[i].wait()
         with scope("pv"):
-            for s in range(i * per, (i + 1) * per, 2):
+            for s in range(start, stop, 2):
                 g = s // group
                 both = jnp.concatenate([vm.cache_values[s], vm.cache_values[s + 1]], axis=1)
                 got = dot(work.mixed[g * group : (g + 1) * group, :], both)
@@ -293,6 +293,10 @@
     rank = dot(named.astype(BF16), before)
     taken = (named > 0.5) & (rank == (slot % 4).astype(F32))
     return jnp.where(taken, 1.0, 0.0).astype(BF16), jnp.where(taken, weight, 0.0)
+
+
+def is_in(e, groups):
+    return sum(1 // (1 + (e - g) * (e - g)) for g in groups)
 
 
 def far_first(sizes):
@@ -354,14 +358,15 @@
     with scope("d1"):
         rows = dot(dispatch, (kept * gain).astype(BF16)).astype(BF16)
         bufs.a[...] = rows.reshape(bufs.a.shape)
+        mine = sum(i * is_in(e, of) for i, of in enumerate(sum(SETS, ())))
         for dz, dx, dy in far_first((n_z, n_x, n_y)):
             to = ep_at(dz, dx)
             if dz or dx or dy:
                 which = 1 if dy else 0
-                send(bufs.a.at[to], bufs.x.at[y, e], sems.x.send.at[which], sems.x.recv.at[e], to, tp_at(dy, 0))
+                send(bufs.a.at[to], bufs.x.at[y, e], sems.x.send.at[which], sems.x.recv.at[mine], to, tp_at(dy, 0))
         bufs.x[y, e] = bufs.a[e]
 
-    halves = (EARLY, [g for g in range(n_ep) if g not in EARLY])
+    halves = (EARLY, sum(SETS[1], ()))
     hids = (bufs.hid_a, bufs.hid_b)
     ff = vm.gate_up_w.shape[2] // 2
 
@@ -390,23 +395,35 @@
         ]
         return of_expert(got), squares
 
+    def collect(h):
+        for of in SETS[h]:
+            place = sum(SETS, ()).index(of)
+            copies = n_y * len(of)
+
+            @pl.when(is_in(e, of) == 0)
+            def _():
+                arrive(bufs.x.at[0, pl.ds(0, copies)], sems.x.recv.at[place])
+
+            @pl.when(is_in(e, of) == 1)
+            def _():
+                arrive(bufs.x.at[0, pl.ds(0, copies - 1)], sems.x.recv.at[place])
+
+            for g in of:
+                send(bufs.x.at[:, g], bufs.p.at[:, g], sems.p.send.at[0], sems.p.recv.at[h], e, partner)
+
     for h, groups in enumerate(halves):
-        with scope("xw"):
-            for g in groups:
-
-                @pl.when(e != g)
-                def _():
-                    arrive(bufs.x.at[pl.ds(0, n_y), g], sems.x.recv.at[g])
-
-                @pl.when(e == g)
-                def _():
-                    arrive(bufs.x.at[pl.ds(0, n_y - 1), g], sems.x.recv.at[g])
-
-                send(bufs.x.at[:, g], bufs.p.at[:, g], sems.p.send.at[0], sems.p.recv.at[h], e, partner)
         if h == 0:
+            with scope("xw"):
+                collect(0)
             wait(loads.gate_up_w + loads.down_w)
+        else:
+            with scope("xb"):
+                pl.when(c == 0)(lambda: collect(1))
         with scope("gu"):
             first, first_squares = gate_up(bufs.x, c, groups)
+        if h == 0:
+            with scope("xc"):
+                pl.when(c == 1)(lambda: collect(1))
         with scope("pw"):
             arrive(bufs.p.at[:, pl.ds(0, len(groups))], sems.p.recv.at[h])
         with scope("gv"):
@@ -421,7 +438,7 @@
 
             for (dy,) in far_first((n_y,)):
                 if dy:
-                    place = (h * (n_y - 1) + dy - 1) * 2 + c
+                    place = h * (n_y - 1) + dy - 1
                     send(mine, mine, sems.hy.send.at[h], sems.hy.recv.at[place], e, tp_at(dy, 1 - c))
             send(mine, mine, sems.hd.send.at[h], sems.hd.recv.at[h], e, partner)
     for h, groups in enumerate(halves):
@@ -430,9 +447,9 @@
             @pl.when(c == 1)
             def _():
                 for (dy,) in reversed(far_first((n_y,))):
-                    for core in (1, 0) if dy else ():
-                        block = hids[h].at[tp_at(dy, core - c)]
-                        arrive(block, sems.hy.recv.at[(h * (n_y - 1) + n_y - dy - 1) * 2 + core])
+                    if dy:
+                        block = hids[h].at[pl.ds((y + dy) % n_y * 2, 2)]
+                        arrive(block, sems.hy.recv.at[h * (n_y - 1) + n_y - dy - 1])
                         send(block, block, sems.hd.send.at[h], sems.hd.recv.at[h], e, partner)
                 arrive(hids[h].at[0], sems.hd.recv.at[h])
 
@@ -505,9 +522,9 @@
     return Sems(
         idle=pltpu.SemaphoreType.DMA((1,)),
         rs=pair(1, 1),
-        x=pair(2, n_ep),
+        x=pair(2, len(sum(SETS, ()))),
         p=pair(1, 2),
-        hy=pair(2, 2 * (n_tp - 2)),
+        hy=pair(2, n_tp - 2),
         hd=pair(2, 2),
         re=pair(1, 1),
     )

time: 37.2 us -> 36.6 us (0.984); the launches traced: 36.6 us -> 36.5 us
  no operation moved by 1% of the time
where the time goes in v6:
time: 36.6 us; the launch traced here: 36.5 us
  Pallas kernels  35.2 us (96%)
  between operations  0.66 us (2%)
  other arithmetic  0.61 us (2%)
    pallas_call x1, Pallas kernels, run(): pl.pallas_call(kernel, out_shape=pltpu.VMEM((seqs, cols), OUT), in_specs=...  35.2 us

profile of v6, /device:TPU:0, one launch (start us, length us, event | category | flops | bytes accessed | tf_op | source)
XLA Modules:
  0.0 36.5 jit_solution(2679483435080717743)
XLA Ops:
  0.7 35.2 %shard_map.181 = f32[32,256]{1,0:T(8,128)S(1)} custom-call(bf16[32,2048]{1,0:T(8,128)(2,1)} %hbm_tokens.1, s32[1,32]{1,0:T(1,128)} %bitcast.20, bf16[32,1024,128]{2,1,0:T(8,128)(2,1)} %hbm_cache_keys.1, bf16[32,1024,128]{2,1,0:T(8,128)(2,1)} %hbm_cache_values.1, f32[1,2048]{1,0:T(1,128)} %bitcast.16, bf16[64,2048]{1,0:T(8,128)(2,1)} %bitcast.12, ...), custom_call_target="tpu_custom_call" | custom-call | tf_op jit(solution)/shard_map/pallas_call | solution.py:596
  35.8 0.6 %convert_element_type.3 = bf16[32,256]{1,0:T(8,128)(2,1)} convert(f32[32,256]{1,0:T(8,128)S(1)} %shard_map.181) | non-fusion elementwise | flops 8192 | bytes 49152 | tf_op jit(solution)/shard_map/convert_element_type | solution.py:622

commit v7 on v6

--- a/solution.py
+++ b/solution.py
@@ -69,11 +69,11 @@
     lengths: Any
     mix_lambda: Any
     head_gain: Any
-    value_w: Any
     ffn_gain: Any
     routes: Any
     route_logits: Any
     keys: Any
+    value_w: Any
     values: Any
     out_w: Any
     gate_up_w: Any
@@ -164,11 +164,11 @@
         lengths=copy(hbm.lengths, vm.lengths),
         mix_lambda=copy(hbm.mix_lambda, vm.mix_lambda),
         head_gain=copy(hbm.head_gain, vm.head_gain),
-        value_w=copy(hbm.value_w, vm.value_w),
         ffn_gain=copy(hbm.ffn_gain, vm.ffn_gain),
         routes=copy(hbm.routes, vm.routes),
         route_logits=copy(hbm.route_logits, vm.route_logits),
         keys=sum((copy(hbm.cache_keys.at[:, s, :], vm.cache_keys.at[:, s, :]) for s in spans), ()),
+        value_w=copy(hbm.value_w, vm.value_w),
         values=sum((copy(hbm.cache_values.at[b], vm.cache_values.at[b]) for b in blocks), ()),
         out_w=copy(hbm.out_w, vm.out_w),
         gate_up_w=(
@@ -299,6 +299,11 @@
     return sum(1 // (1 + (e - g) * (e - g)) for g in groups)
 
 
+def runs(groups):
+    firsts = [g for g in groups if g - 1 not in groups]
+    return [(g, next(n for n in itertools.count(1) if g + n not in groups)) for g in firsts]
+
+
 def far_first(sizes):
     every = [()]
     for n in sizes:
@@ -408,8 +413,9 @@
             def _():
                 arrive(bufs.x.at[0, pl.ds(0, copies - 1)], sems.x.recv.at[place])
 
-            for g in of:
-                send(bufs.x.at[:, g], bufs.p.at[:, g], sems.p.send.at[0], sems.p.recv.at[h], e, partner)
+            for first, count in runs(of):
+                at = pl.ds(first, count)
+                send(bufs.x.at[:, at], bufs.p.at[:, at], sems.p.send.at[0], sems.p.recv.at[h], e, partner)
 
     for h, groups in enumerate(halves):
         if h == 0:

time: 36.6 us -> 36.5 us (level)
  no operation moved by 1% of the time
where the time goes in v7:
time: 36.5 us; the launch traced here: 36.4 us
  Pallas kernels  35.2 us (96%)
  between operations  0.66 us (2%)
  other arithmetic  0.61 us (2%)
    pallas_call x1, Pallas kernels, run(): pl.pallas_call(kernel, out_shape=pltpu.VMEM((seqs, cols), OUT), in_specs=...  35.2 us

profile of v7, /device:TPU:0, one launch (start us, length us, event | category | flops | bytes accessed | tf_op | source)
XLA Modules:
  0.0 36.4 jit_solution(257925379126644171)
XLA Ops:
  0.7 35.2 %shard_map.181 = f32[32,256]{1,0:T(8,128)S(1)} custom-call(bf16[32,2048]{1,0:T(8,128)(2,1)} %hbm_tokens.1, s32[1,32]{1,0:T(1,128)} %bitcast.20, bf16[32,1024,128]{2,1,0:T(8,128)(2,1)} %hbm_cache_keys.1, bf16[32,1024,128]{2,1,0:T(8,128)(2,1)} %hbm_cache_values.1, f32[1,2048]{1,0:T(1,128)} %bitcast.16, bf16[64,2048]{1,0:T(8,128)(2,1)} %bitcast.12, ...), custom_call_target="tpu_custom_call" | custom-call | tf_op jit(solution)/shard_map/pallas_call | solution.py:602
  35.8 0.6 %convert_element_type.3 = bf16[32,256]{1,0:T(8,128)(2,1)} convert(f32[32,256]{1,0:T(8,128)S(1)} %shard_map.181) | non-fusion elementwise | flops 8192 | bytes 49152 | tf_op jit(solution)/shard_map/convert_element_type | solution.py:628
